TPU v7x, 32 devices: a whole 2x2x4 slice. The times are simulated.
32 devices in a mesh: kv: 16 (over z, y, core), tp: 2 (over x).
Axes of the slice: x: 2, y: 2, z: 4, core: 2. Of those that a mesh axis runs over, the one named last changes fastest.
Arguments:
- hidden_rows: bfloat16 [6144, 2048], P('kv'), may hold values from -6 to 6
- proj_query: bfloat16 [2048, 2048], P(None, 'tp'), may hold values from -0.125 to 0.125
- proj_key: bfloat16 [2048, 256], P(None, 'tp'), may hold values from -0.125 to 0.125
- proj_value: bfloat16 [2048, 256], P(None, 'tp'), may hold values from -0.125 to 0.125
- proj_output: bfloat16 [2048, 2048], P('tp'), may hold values from -0.125 to 0.125
- head_scale: float32 [32], P('tp'), may hold values from 0.25 to 96
- hot_blocks: int32 [16], replicated, may hold values from 0 to 191, as said below
- chosen_blocks: int32 [96, 16], P('kv'), may hold values from 0 to 27, as said below
Outputs:
- layer_out: bfloat16 [6144, 2048], P('kv', 'tp')
Inputs may be any that keep to these rules, and one draw needn't show every extreme that they name: `hot_blocks`: 16 different key-block numbers; no device's 12 key blocks hold more than 2 of them, and in every draw some device holds exactly 2. `chosen_blocks`: each row's 16 codes name different key blocks; among them are the key blocks that cover the positions of query block b; no code of 12 or more names a block on the query block's own device.
All inputs are finite; a program needn't handle non-finite values.
Results may differ from a plain program's by a relative error of at most 0.01.
The roundings to bfloat16 on the way count: a program that leaves them out, or rounds other values in their place, can miss the bound.
Values may be sent and summed in bfloat16 or wider, within the bound.
No kernel may reach another device: no remote copies, remote signals or barrier semaphores. Data moves between devices by JAX's collectives and lax.ppermute only.
A program may use at most 64 MiB of HBM per device.

v0:
```python
import jax
import jax.numpy as jnp
from jax import lax
from jax.sharding import PartitionSpec as P

HD = 64
KB = 32
QB = 64
NSEL = 16
NHOT = 16
HOT_MOST = 2


def local(
    hidden_rows,
    proj_query,
    proj_key,
    proj_value,
    proj_output,
    head_scale,
    hot_blocks,
    chosen_blocks,
):
    device = lax.axis_index("kv")
    tok_rows = hidden_rows.shape[0]
    own_blocks = tok_rows // KB
    kv_heads = proj_key.shape[1] // HD
    head_count = proj_query.shape[1] // HD
    group_size = head_count // kv_heads
    width = 2 * kv_heads * HD
    queries = jnp.dot(hidden_rows, proj_query, preferred_element_type=jnp.float32).astype(
        jnp.bfloat16
    )
    both_proj = jnp.concatenate([proj_key, proj_value], axis=1)
    packed = jnp.dot(hidden_rows, both_proj, preferred_element_type=jnp.float32).astype(
        jnp.bfloat16
    )
    packed = packed.reshape(own_blocks, KB, width)
    owners = hot_blocks // own_blocks
    offsets = hot_blocks - owners * own_blocks
    is_mine = owners == device
    selector = (offsets[:, None] == jnp.arange(own_blocks, dtype=jnp.int32)[None, :]) & is_mine[
        :, None
    ]
    hot_range = jnp.arange(NHOT, dtype=jnp.int32)
    before = hot_range[None, :] < hot_range[:, None]
    ranking = jnp.sum(((owners[None, :] == owners[:, None]) & before).astype(jnp.int32), axis=1)
    slot_of = owners * HOT_MOST + ranking
    slot_mask = (ranking[None, :] == jnp.arange(HOT_MOST, dtype=jnp.int32)[:, None]) & is_mine[
        None, :
    ]
    slot_pick = jnp.dot(
        slot_mask.astype(jnp.bfloat16),
        selector.astype(jnp.bfloat16),
        preferred_element_type=jnp.float32,
    ).astype(jnp.bfloat16)
    packed_slots = jnp.einsum(
        "sn,nkw->skw", slot_pick, packed, preferred_element_type=jnp.float32
    ).astype(jnp.bfloat16)
    piece = lax.all_gather(packed_slots, "kv", axis=0, tiled=True)
    piece_rows = piece.shape[0]
    match = slot_of[:, None] == jnp.arange(piece_rows, dtype=jnp.int32)[None, :]
    added = jnp.einsum(
        "hm,mkw->hkw", match.astype(jnp.bfloat16), piece, preferred_element_type=jnp.float32
    ).astype(jnp.bfloat16)
    pool = jnp.concatenate([packed, added], axis=0)
    hot_match = (
        chosen_blocks[:, :, None] - own_blocks == jnp.arange(NHOT, dtype=jnp.int32)[None, None, :]
    )
    hot_global = jnp.sum(jnp.where(hot_match, hot_blocks[None, None, :], 0), axis=2)
    global_ids = jnp.where(
        chosen_blocks < own_blocks, device * own_blocks + chosen_blocks, hot_global
    )
    query_blocks = tok_rows // QB
    gathered = jnp.take(pool, chosen_blocks, axis=0).reshape(
        query_blocks, NSEL * KB, 2 * kv_heads, HD
    )
    key_rows = gathered[:, :, :kv_heads]
    value_rows = gathered[:, :, kv_heads:]
    grouped_query = queries.reshape(query_blocks, QB, kv_heads, group_size, HD)
    scores = jnp.einsum(
        "bqcgd,blcd->bcgql", grouped_query, key_rows, preferred_element_type=jnp.float32
    ) * HD ** (-0.5)
    scores = scores * head_scale.reshape(kv_heads, group_size)[None, :, :, None, None]
    query_pos = device * tok_rows + jnp.arange(tok_rows, dtype=jnp.int32).reshape(query_blocks, QB)
    key_pos = global_ids[:, :, None] * KB + jnp.arange(KB, dtype=jnp.int32)[None, None, :]
    key_pos = key_pos.reshape(query_blocks, NSEL * KB)
    visible = key_pos[:, None, :] <= query_pos[:, :, None]
    scores = jnp.where(visible[:, None, None], scores, -jnp.inf)
    row_max = jnp.max(scores, axis=-1, keepdims=True)
    lifted = jnp.exp(scores - row_max)
    weights = (lifted / jnp.sum(lifted, axis=-1, keepdims=True)).astype(jnp.bfloat16)
    attended = jnp.einsum(
        "bcgql,blcd->bqcgd", weights, value_rows, preferred_element_type=jnp.float32
    ).astype(jnp.bfloat16)
    attended = attended.reshape(tok_rows, head_count * HD)
    partial_value = jnp.dot(attended, proj_output, preferred_element_type=jnp.float32)
    return lax.psum_scatter(
        partial_value.astype(jnp.bfloat16), "tp", scatter_dimension=1, tiled=True
    )


def solution(mesh):
    return jax.shard_map(
        local,
        mesh=mesh,
        in_specs=(
            P("kv", None),
            P(None, "tp"),
            P(None, "tp"),
            P(None, "tp"),
            P("tp", None),
            P("tp"),
            P(),
            P("kv", None),
        ),
        out_specs=P("kv", "tp"),
        check_vma=False,
    )
```

profile of v0, /device:TPU:0, one launch (start us, length us, event | category | flops | bytes accessed | tf_op | source)
XLA Modules:
  0.0 121.0 jit_solution(15049854181486884017)
XLA Ops:
  6.5 0.8 compare_and_fusion
  7.4 0.7 broadcast_add_fusion.1
  8.0 0.7 broadcast_multiply_fusion
  8.8 0.7 broadcast_compare_fusion.1
  9.6 0.7 multiply_add_fusion
  10.3 0.9 select_reduce_fusion
  11.2 0.7 select_multiply_fusion
  12.4 2.0 %fusion.10 = bf16[384,256]{0,1:T(8,128)(2,1)S(1)} fusion(bf16[384,2048]{1,0:T(8,128)(2,1)S(1)} %copy-done, bf16[2048,128]{1,0:T(8,128)(2,1)} %param.11, bf16[2048,128]{1,0:T(8,128)(2,1)} %param.10), kind=kOutput, calls=%fused_computation.19 | convolution fusion | flops 404848640 | bytes 2818048 | tf_op jit(solution)/shard_map/dot_general | solution.py:35
  15.0 24.6 %all_gather.3 = bf16[32,32,256]{2,1,0:T(8,128)(2,1)S(1)} all-gather(bf16[2,32,256]{2,1,0:T(8,128)(2,1)S(1)} %copy.28), channel_id=1, replica_groups=mesh['kv'=16,'tp'=2] {'kv'}, dimensions={0}, use_global_device_ids=true | all-gather | bytes 557056 | tf_op jit(solution)/shard_map/all_gather | solution.py:60
  39.6 0.4 convolution_convert_fusion.2
  40.5 4.0 %convolution_convert_fusion.1 = bf16[384,1024]{1,0:T(8,128)(2,1)S(1)} fusion(bf16[384,2048]{1,0:T(8,128)(2,1)S(1)} %copy-done, bf16[2048,1024]{1,0:T(8,128)(2,1)} %param.9), kind=kOutput, calls=%fused_computation.16 | convolution fusion | flops 1611005952 | bytes 6553600 | tf_op jit(solution)/shard_map/dot_general | solution.py:31
  44.5 2.1 %reshape.69 = bf16[6,64,2,8,64]{4,3,2,1,0:T(8,128)(2,1)} reshape(bf16[384,1024]{1,0:T(8,128)(2,1)S(1)} %convolution_convert_fusion.1) | data formatting | bytes 1572864 | tf_op jit(solution)/shard_map/reshape | solution.py:80
  46.5 1.9 %gather_fusion = bf16[96,32,256]{2,1,0:T(8,128)(2,1)} fusion(bf16[28,32,256]{2,1,0:T(8,128)(2,1)S(1)} %copy.31, s32[1024]{0:T(1024)S(1)} %pad_clamp_fusion), kind=kCustom, calls=%fused_computation | custom fusion | bytes 3146112 | tf_op jit(solution)/shard_map/jit(_take)/gather | solution.py:75
  48.5 5.8 %gather.7 = bf16[6,512,4,64]{3,2,1,0:T(4,128)(2,1)} reshape(bf16[96,32,256]{2,1,0:T(8,128)(2,1)} %gather_fusion) | data formatting | bytes 3145728 | tf_op jit(solution)/shard_map/jit(_take)/gather | solution.py:75
  54.2 5.6 %copy.32 = bf16[6,512,4,64]{1,3,2,0:T(8,128)(2,1)} copy(bf16[6,512,4,64]{3,2,1,0:T(4,128)(2,1)} %gather.7) | data formatting | bytes 3145728 | tf_op jit(solution)/shard_map/jit(_take)/gather | solution.py:75
  60.0 1.6 %broadcast_select_fusion = bf16[6,512,4,64]{1,3,2,0:T(8,128)(2,1)S(1)} fusion(bf16[6,512,4,64]{1,3,2,0:T(8,128)(2,1)} %copy.32, pred[6,512]{1,0:T(8,128)(4,1)S(1)} %broadcast_in_dim.41), kind=kLoop, calls=%fused_computation.14 | loop fusion | flops 786432 | bytes 3148800 | tf_op jit(solution)/shard_map/jit(_take)/select_n | solution.py:75
  61.6 1.2 copy-done.2
  62.8 1.8 %fusion.7 = f32[6,2,512,64,8]{2,3,4,1,0:T(8,128)S(1)} fusion(bf16[6,64,2,8,64]{4,3,2,1,0:T(8,128)(2,1)S(1)} %copy-done.1, bf16[6,512,4,64]{1,3,2,0:T(8,128)(2,1)S(1)} %broadcast_select_fusion), kind=kOutput, calls=%fused_computation.12 | convolution fusion | flops 402653184 | bytes 14942208 | tf_op jit(solution)/shard_map/bqcgd,blcd->bcgql/dot_general | solution.py:81
  64.6 9.1 %fusion.36 = (f32[6,2,8,64]{3,2,1,0:T(8,128)S(1)}, f32[6,2,8,64,512]{4,3,2,1,0:T(8,128)}) fusion(f32[6,2,512,64,8]{2,3,4,1,0:T(8,128)S(1)} %fusion.7, f32[2,8]{1,0:T(2,128)S(1)} %mul.46, pred[6,64,512]{2,1,0:T(8,128)(4,1)S(1)} %broadcast_compare_fusion), kind=kOutput, calls=%fused_computation.62 | output fusion | flops 18874880 | bytes 25387072 | tf_op jit(solution)/shard_map/sub | solution.py:91
  73.7 7.2 %fusion.9 = bf16[6,64,2,8,64]{1,4,3,2,0:T(8,128)(2,1)} fusion(f32[6,2,8,64,512]{4,3,2,1,0:T(8,128)} %get-tuple-element.12, f32[6,2,8,64]{3,2,1,0:T(8,128)S(1)} %get-tuple-element.11, bf16[6,512,4,64]{1,3,2,0:T(8,128)(2,1)S(1)} %copy-done.3), kind=kOutput, calls=%fused_computation.15 | convolution fusion | flops 409337856 | bytes 14204928 | tf_op jit(solution)/shard_map/bcgql,blcd->bqcgd/dot_general | solution.py:93
  80.9 2.4 %copy.34 = bf16[6,64,2,8,64]{4,3,2,1,0:T(8,128)(2,1)S(1)} copy(bf16[6,64,2,8,64]{1,4,3,2,0:T(8,128)(2,1)} %fusion.9) | data formatting | bytes 1572864 | tf_op jit(solution)/shard_map/convert_element_type | solution.py:95
  83.3 1.9 %reshape.70 = bf16[384,1024]{1,0:T(8,128)(2,1)} reshape(bf16[6,64,2,8,64]{4,3,2,1,0:T(8,128)(2,1)S(1)} %copy.34) | data formatting | bytes 1572864 | tf_op jit(solution)/shard_map/reshape | solution.py:96
  85.2 5.4 %convolution_convert_fusion = bf16[384,2048]{1,0:T(8,128)(2,1)} fusion(bf16[384,1024]{1,0:T(8,128)(2,1)} %reshape.70, bf16[1024,2048]{1,0:T(8,128)(2,1)} %param.12), kind=kOutput, calls=%fused_computation.10 | convolution fusion | flops 1611399168 | bytes 6553600 | tf_op jit(solution)/shard_map/dot_general | solution.py:97
  90.6 23.6 %reduce-scatter.2.cloned.1.call-done = bf16[384,1024]{1,0:T(8,128)(2,1)} async-done(((bf16[384,2048]{1,0:T(8,128)(2,1)}), bf16[384,1024]{1,0:T(8,128)(2,1)}) %reduce-scatter.2.cloned.1.call-update) | async-done | bytes 786448 | tf_op jit(solution)/shard_map/reduce_scatter | solution.py:98
  (28 shorter events, 2.0 us)
Async XLA Ops:
  6.5 5.9 %copy-start = (bf16[384,2048]{1,0:T(8,128)(2,1)S(1)}, bf16[384,2048]{1,0:T(8,128)(2,1)}, u32[]{:S(2)}) copy-start(bf16[384,2048]{1,0:T(8,128)(2,1)} %param.8) | copy-start | bytes 4718596
  6.5 107.6 %reduce-scatter.2.cloned.1.call-start = ((), (), s32[]{:S(2)}) async-start(), calls=%async_computation.1 | async-start | bytes 2359296 | tf_op jit(solution)/shard_map/reduce_scatter | solution.py:98
  54.2 8.6 %copy-start.1 = (bf16[6,64,2,8,64]{4,3,2,1,0:T(8,128)(2,1)S(1)}, bf16[6,64,2,8,64]{4,3,2,1,0:T(8,128)(2,1)}, u32[]{:S(2)}) copy-start(bf16[6,64,2,8,64]{4,3,2,1,0:T(8,128)(2,1)} %reshape.69) | copy-start | bytes 2359300
  61.6 1.2 copy-start.2
  64.6 9.1 %copy-start.3 = (bf16[6,512,4,64]{1,3,2,0:T(8,128)(2,1)S(1)}, bf16[6,512,4,64]{1,3,2,0:T(8,128)(2,1)}, u32[]{:S(2)}) copy-start(bf16[6,512,4,64]{1,3,2,0:T(8,128)(2,1)} %copy-done.2) | copy-start | bytes 4718596
Sparse Core Ops, SparseCore 0:
  90.7 23.3 reduce-scatter.1
where the time goes:
time: 122 us; the launch traced here: 121 us
  blocking collectives  24.6 us (20%)
  waiting for transfers between devices  23.6 us (19%)
  local copies, waits for them, and re-layouts  22 us (18%)
  matrix products  21 us (17%)
  other arithmetic  16.3 us (13%)
  between operations  13.5 us (11%)
    all_gather x1, blocking collectives, local(): piece = lax.all_gather(packed_slots, 'kv', axis=0, tiled=True)  24.6 us
    reduce_scatter x1, waiting for transfers between devices, local(): lax.psum_scatter(partial_value.astype(jnp.bfloat16), 'tp', scatter_dimens...  23.6 us
    gather x3, local copies, waits for them, and re-layouts, local(): jnp.take(pool, chosen_blocks, axis=0)  13.3 us
    sub x1, other arithmetic, local(): lifted = jnp.exp(scores - row_max)  9.09 us
    dot_general x1, matrix products, local(): jnp.einsum('bcgql,blcd->bqcgd', weights, value_rows, preferred_element_ty...  7.22 us
    dot_general x1, matrix products, local(): jnp.dot(attended, proj_output, preferred_element_type=jnp.float32)  5.38 us
    dot_general x1, matrix products, local(): jnp.dot(hidden_rows, proj_query, preferred_element_type=jnp.float32)  3.98 us
  transfers between devices with their start and end apart: 1, of which 1 were waited for; matrix products, arithmetic and copies ran while one was open for 0% of the time, Pallas kernels for 0%

commit v1 on v0

v1 whole, which is shorter than its diff:
```python
import functools

import jax
import jax.numpy as jnp
from jax import lax
from jax.experimental import pallas as pl
from jax.experimental.pallas import tpu as pltpu
from jax.sharding import PartitionSpec as P

HD = 64
KB = 32
QB = 64
NSEL = 16
NHOT = 16
HOT_MOST = 2


def exchange_steps(count):
    steps = []
    step = 2
    while step < count:
        steps.append(step)
        step *= 2
    if count > 1:
        steps.append(1)
    return steps


def slot_kernel(hot, hidden, wk, wv, slots, table, rows, sem, *, own_blocks, steps):
    me = lax.axis_index("kv")
    owners = [lax.div(hot[h], own_blocks) for h in range(NHOT)]
    offs = [jnp.int32(0), jnp.int32(0)]
    ranks = []
    for h in range(NHOT):
        rank = jnp.int32(0)
        for g in range(h):
            rank = rank + jnp.where(owners[g] == owners[h], 1, 0)
        ranks.append(rank)
        mine = owners[h] == me
        for r in range(HOT_MOST):
            offs[r] = jnp.where(mine & (rank == r), hot[h] - owners[h] * own_blocks, offs[r])
    copies = []
    for r in range(HOT_MOST):
        copy = pltpu.make_async_copy(
            hidden.at[pl.ds(pl.multiple_of(offs[r] * KB, KB), KB)],
            rows.at[pl.ds(r * KB, KB)],
            sem.at[r],
        )
        copy.start()
        copies.append(copy)
    for h in range(NHOT):
        apart = owners[h] ^ me
        place = jnp.int32(0)
        for j, step in enumerate(steps):
            place = place + jnp.where((apart & step) != 0, 1 << j, 0)
        table[h] = (own_blocks + place * HOT_MOST + ranks[h]) * KB
    for copy in copies:
        copy.wait()
    x = rows[...]
    half = wk.shape[1]
    slots[:, :half] = jnp.dot(x, wk[...], preferred_element_type=jnp.float32).astype(jnp.bfloat16)
    slots[:, half:] = jnp.dot(x, wv[...], preferred_element_type=jnp.float32).astype(jnp.bfloat16)


def attend_kernel(
    codes,
    hot,
    table,
    scale,
    q,
    keys,
    values,
    near,
    far,
    wo,
    att,
    *rest,
    first,
    count,
    n_tp,
):
    *sends, pool, picked, s_buf, p_buf, wo_buf, sem = rest
    me = lax.axis_index("kv")
    here = lax.axis_index("tp")
    part = wo_buf.shape[2]
    loads = []
    for d in range(1, n_tp):
        there = lax.rem(here + d, n_tp)
        load = pltpu.make_async_copy(
            wo.at[:, pl.ds(pl.multiple_of(there * part, part), part)],
            wo_buf.at[d - 1],
            sem.at[d - 1],
        )
        load.start()
        loads.append(load)
    tok_rows, kw = keys.shape
    own_blocks = tok_rows // KB
    kv_heads = kw // HD
    group = q.shape[1] // HD // kv_heads
    near_rows = near.shape[0]
    pool[:tok_rows, :kw] = keys[...]
    pool[:tok_rows, kw:] = values[...]
    pool[tok_rows : tok_rows + near_rows, :] = near[...]
    pool[tok_rows + near_rows :, :] = far[...]
    lane = lax.broadcasted_iota(jnp.int32, (1, NSEL * KB), 1)
    lane_block = lane // KB
    for b in range(count):
        key_pos = lane - lane_block * KB
        for e in range(NSEL):
            code = codes[first + b, e]
            hot_at = jnp.maximum(code - own_blocks, 0)
            is_own = code < own_blocks
            row = jnp.where(is_own, code * KB, table[hot_at])
            block = jnp.where(is_own, me * own_blocks + code, hot[hot_at])
            key_pos = key_pos + jnp.where(lane_block == e, block * KB, 0)
            picked[e * KB : (e + 1) * KB, :] = pool[pl.ds(pl.multiple_of(row, KB), KB), :]
        query_pos = (
            me * tok_rows + (first + b) * QB + lax.broadcasted_iota(jnp.int32, (QB, 1), 0)
        )
        bias = jnp.where(key_pos <= query_pos, 0.0, -jnp.inf).astype(jnp.float32)
        for c in range(kv_heads):
            heads = [c * group + g for g in range(group)]
            q_rows = jnp.concatenate(
                [q[b * QB : (b + 1) * QB, h * HD : (h + 1) * HD] for h in heads], axis=0
            )
            s_buf[...] = lax.dot_general(
                q_rows,
                picked[:, c * HD : (c + 1) * HD],
                (((1,), (1,)), ((), ())),
                preferred_element_type=jnp.float32,
            )
            sums = []
            for g, h in enumerate(heads):
                at = slice(g * QB, (g + 1) * QB)
                s = s_buf[at, :] * (scale[h] * HD ** (-0.5)) + bias
                lifted = jnp.exp(s - jnp.max(s, axis=-1, keepdims=True))
                sums.append(jnp.sum(lifted, axis=-1, keepdims=True))
                p_buf[at, :] = lifted.astype(jnp.bfloat16)
            out = jnp.dot(
                p_buf[...],
                picked[:, kw + c * HD : kw + (c + 1) * HD],
                preferred_element_type=jnp.float32,
            )
            for g, h in enumerate(heads):
                att[b * QB : (b + 1) * QB, h * HD : (h + 1) * HD] = (
                    out[g * QB : (g + 1) * QB, :] / sums[g]
                ).astype(jnp.bfloat16)
    for d, send in enumerate(sends):
        loads[d].wait()
        send[...] = jnp.dot(att[...], wo_buf[d], preferred_element_type=jnp.float32).astype(
            jnp.bfloat16
        )


def own_kernel(*refs):
    *atts, wo, out, wo_buf, sem = refs
    half = wo_buf.shape[1]
    here = lax.axis_index("tp")
    load = pltpu.make_async_copy(
        wo.at[:, pl.ds(pl.multiple_of(here * half, half), half)], wo_buf, sem
    )
    load.start()
    load.wait()
    at = 0
    for a in atts:
        rows = a.shape[0]
        out[at : at + rows, :] = jnp.dot(
            a[...], wo_buf[...], preferred_element_type=jnp.float32
        ).astype(jnp.bfloat16)
        at += rows


def local(
    hidden_rows,
    proj_query,
    proj_key,
    proj_value,
    proj_output,
    head_scale,
    hot_blocks,
    chosen_blocks,
    *,
    n_kv,
    n_tp,
):
    tok_rows = hidden_rows.shape[0]
    own_blocks = tok_rows // KB
    kw = proj_key.shape[1]
    width = 2 * kw
    heads_w = proj_query.shape[1]
    part = proj_output.shape[1] // n_tp
    query_blocks = tok_rows // QB
    steps = exchange_steps(n_kv)
    smem = pl.BlockSpec(memory_space=pltpu.SMEM)
    vmem = pl.BlockSpec(memory_space=pltpu.VMEM)
    anym = pl.BlockSpec(memory_space=pl.ANY)
    slot_rows = HOT_MOST * KB
    slots, table = pl.pallas_call(
        functools.partial(slot_kernel, own_blocks=own_blocks, steps=steps),
        out_shape=(
            jax.ShapeDtypeStruct((slot_rows, width), jnp.bfloat16),
            jax.ShapeDtypeStruct((NHOT,), jnp.int32),
        ),
        in_specs=[smem, anym, vmem, vmem],
        out_specs=(vmem, smem),
        scratch_shapes=[
            pltpu.VMEM((slot_rows, hidden_rows.shape[1]), jnp.bfloat16),
            pltpu.SemaphoreType.DMA((HOT_MOST,)),
        ],
        name="slot_rows",
    )(hot_blocks, hidden_rows, proj_key, proj_value)

    def swap(x, step):
        return lax.ppermute(x, "kv", [(i, i ^ step) for i in range(n_kv)])

    near = slots
    for step in steps[:-1]:
        near = jnp.concatenate([near, swap(near, step)], axis=0)
    far = swap(near, steps[-1])

    def project(w):
        return jnp.dot(hidden_rows, w, preferred_element_type=jnp.float32).astype(jnp.bfloat16)

    queries = project(proj_query)
    keys = project(proj_key)
    values = project(proj_value)
    sizes = [1, 1] + [2] * ((query_blocks - 2) // 2)
    first = 0
    atts = []
    received = [[] for _ in range(1, n_tp)]
    group_rows = heads_w // HD // (kw // HD) * QB
    for count in sizes:
        rows = count * QB
        att, *sends = pl.pallas_call(
            functools.partial(attend_kernel, first=first, count=count, n_tp=n_tp),
            out_shape=[jax.ShapeDtypeStruct((rows, heads_w), jnp.bfloat16)]
            + [jax.ShapeDtypeStruct((rows, part), jnp.bfloat16)] * (n_tp - 1),
            in_specs=[smem, smem, smem, smem, vmem, vmem, vmem, vmem, vmem, anym],
            out_specs=[vmem] * n_tp,
            scratch_shapes=[
                pltpu.VMEM((tok_rows + near.shape[0] + far.shape[0], width), jnp.bfloat16),
                pltpu.VMEM((NSEL * KB, width), jnp.bfloat16),
                pltpu.VMEM((group_rows, NSEL * KB), jnp.float32),
                pltpu.VMEM((group_rows, NSEL * KB), jnp.bfloat16),
                pltpu.VMEM((n_tp - 1, proj_output.shape[0], part), jnp.bfloat16),
                pltpu.SemaphoreType.DMA((n_tp - 1,)),
            ],
            name="attend",
        )(
            chosen_blocks,
            hot_blocks,
            table,
            head_scale,
            queries[first * QB : first * QB + rows],
            keys,
            values,
            near,
            far,
            proj_output,
        )
        atts.append(att)
        for d, send in enumerate(sends):
            pairs = [(i, (i + d + 1) % n_tp) for i in range(n_tp)]
            received[d].append(lax.ppermute(send, "tp", pairs))
        first += count
    own = pl.pallas_call(
        own_kernel,
        out_shape=jax.ShapeDtypeStruct((tok_rows, part), jnp.bfloat16),
        in_specs=[vmem] * len(atts) + [anym],
        out_specs=vmem,
        scratch_shapes=[
            pltpu.VMEM((proj_output.shape[0], part), jnp.bfloat16),
            pltpu.SemaphoreType.DMA,
        ],
        name="own_part",
    )(*atts, proj_output)
    total = own.astype(jnp.float32)
    for pieces in received:
        total = total + jnp.concatenate(pieces, axis=0).astype(jnp.float32)
    return total.astype(jnp.bfloat16)


def solution(mesh):
    return jax.shard_map(
        functools.partial(local, n_kv=mesh.shape["kv"], n_tp=mesh.shape["tp"]),
        mesh=mesh,
        in_specs=(
            P("kv", None),
            P(None, "tp"),
            P(None, "tp"),
            P(None, "tp"),
            P("tp", None),
            P("tp"),
            P(),
            P("kv", None),
        ),
        out_specs=P("kv", "tp"),
        check_vma=False,
    )
```

time: 122 us -> 64.5 us (0.53)
  Pallas kernels: 0 us -> 33.2 us
  blocking collectives: 24.6 us -> 0 us
  local copies, waits for them, and re-layouts: 22 us -> 2.27 us
  waiting for transfers between devices: 23.6 us -> 7.91 us
  matrix products: 21 us -> 6.41 us
  other arithmetic: 16.3 us -> 2.33 us
  between operations: 13.5 us -> 0.15 us
  starting transfers between devices: 0.01 us -> 11.7 us
    pallas_call x0 -> x6, Pallas kernels: none -> 33.2 us  [the longest x4 24.6 us: local(): pl.pallas_call(functools.partial(attend_kernel, first=first, count=count,...]
    all_gather x1 -> x0, blocking collectives: 24.6 us -> none  [local(): piece = lax.all_gather(packed_slots, 'kv', axis=0, tiled=True)]
    reduce_scatter x1 -> x0, waiting for transfers between devices: 23.6 us -> none  [local(): lax.psum_scatter(partial_value.astype(jnp.bfloat16), 'tp', scatter_dimens...]
    dot_general x7 -> x3, matrix products: 21 us -> 6.41 us  [project(): jnp.dot(hidden_rows, w, preferred_element_type=jnp.float32)]
    gather x3 -> x0, local copies, waits for them, and re-layouts: 13.3 us -> none  [local(): jnp.take(pool, chosen_blocks, axis=0)]
    ppermute x0 -> x8, starting transfers between devices: none -> 11.7 us  [the longest x4 7.42 us: swap(): return lax.ppermute(x, 'kv', [(i, i ^ step) for i in range(n_kv)])]
    sub x2 -> x0, other arithmetic: 9.78 us -> none  [the longest x1 9.09 us: local(): lifted = jnp.exp(scores - row_max)]
    ppermute x0 -> x8, waiting for transfers between devices: none -> 7.91 us  [the longest x4 7.9 us: swap(): return lax.ppermute(x, 'kv', [(i, i ^ step) for i in range(n_kv)])]
  transfers between devices with their start and end apart: 1 -> 8, of which waited for: 1 -> 3; matrix products, arithmetic and copies ran while one was open for 0% -> 12% of each run, Pallas kernels for 0% -> 36%
where the time goes in v1:
time: 64.5 us; the launch traced here: 64 us
  Pallas kernels  33.2 us (51%)
  starting transfers between devices  11.7 us (18%)
  waiting for transfers between devices  7.91 us (12%)
  matrix products  6.41 us (10%)
  other arithmetic  2.33 us (4%)
  local copies, waits for them, and re-layouts  2.27 us (4%)
    pallas_call x4, Pallas kernels, local(): pl.pallas_call(functools.partial(attend_kernel, first=first, count=count,...  24.6 us
    ppermute x4, waiting for transfers between devices, swap(): return lax.ppermute(x, 'kv', [(i, i ^ step) for i in range(n_kv)])  7.9 us
    ppermute x4, starting transfers between devices, swap(): return lax.ppermute(x, 'kv', [(i, i ^ step) for i in range(n_kv)])  7.42 us
    dot_general x3, matrix products, project(): jnp.dot(hidden_rows, w, preferred_element_type=jnp.float32)  6.41 us
    pallas_call x1, Pallas kernels, local(): pl.pallas_call(own_kernel, out_shape=jax.ShapeDtypeStruct((tok_rows, part...  5.1 us
    ppermute x4, starting transfers between devices, local(): received[d].append(lax.ppermute(send, 'tp', pairs))  4.32 us
    pallas_call x1, Pallas kernels, local(): pl.pallas_call(functools.partial(slot_kernel, own_blocks=own_blocks, step...  3.55 us
    convert_element_type x1, other arithmetic, local(): return total.astype(jnp.bfloat16)  2.32 us
  transfers between devices with their start and end apart: 8, of which 3 were waited for; matrix products, arithmetic and copies ran while one was open for 12% of the time, Pallas kernels for 36%

profile of v1, /device:TPU:0, one launch (start us, length us, event | category | flops | bytes accessed | tf_op | source)
XLA Modules:
  0.0 64.0 jit_solution(7732643928326538281)
XLA Ops:
  0.0 3.6 %slot_rows.1 = (bf16[64,256]{1,0:T(8,128)(2,1)}, s32[16]{0:T(128)}) custom-call(s32[16]{0:T(128)} %hot.9, bf16[384,2048]{1,0:T(8,128)(2,1)} %hidden.1, bf16[2048,128]{1,0:T(8,128)(2,1)} %wk.1, bf16[2048,128]{1,0:T(8,128)(2,1)} %wv.1), custom_call_target="tpu_custom_call" | custom-call | tf_op jit(solution)/shard_map/slot_rows/pallas_call | solution.py:198
  3.6 3.1 %collective-permute-start = (bf16[64,256]{1,0:T(8,128)(2,1)}, bf16[64,256]{1,0:T(8,128)(2,1)S(1)}, u32[]{:S(2)}, u32[]{:S(2)}) collective-permute-start(bf16[64,256]{1,0:T(8,128)(2,1)} %get-tuple-element.16), channel_id=1, source_target_pairs={{0,4},{2,6},{4,0},{6,2},{8,12},{10,14},{12,8},{14,10},{16,20},{18,... | collective-permute-start | bytes 98312 | tf_op jit(solution)/shard_map/ppermute | solution.py:214
  6.6 1.2 %convolution_convert_fusion.2.keys = bf16[384,128]{1,0:T(8,128)(2,1)} fusion(bf16[384,2048]{1,0:T(8,128)(2,1)S(1)} %copy-done, bf16[2048,128]{1,0:T(8,128)(2,1)S(1)} %copy-done.3), kind=kOutput, calls=%fused_computation.3 | convolution fusion | flops 201375744 | bytes 2195456 | tf_op jit(solution)/shard_map/dot_general | solution.py:222
  7.8 4.0 %convolution_convert_fusion = bf16[384,1024]{1,0:T(8,128)(2,1)S(1)} fusion(bf16[384,2048]{1,0:T(8,128)(2,1)S(1)} %copy-done, bf16[2048,1024]{1,0:T(8,128)(2,1)} %param.9), kind=kOutput, calls=%fused_computation.1 | convolution fusion | flops 1611005952 | bytes 6553600 | tf_op jit(solution)/shard_map/dot_general | solution.py:222
  11.8 0.8 %fusion = (bf16[128,1024]{1,0:T(8,128)(2,1)}, bf16[128,1024]{1,0:T(8,128)(2,1)}) fusion(bf16[384,1024]{1,0:T(8,128)(2,1)S(1)} %convolution_convert_fusion), kind=kLoop, calls=%fused_computation.10 | loop fusion | bytes 1048576 | tf_op jit(solution)/shard_map/slice | solution.py:254
  12.7 1.6 %collective-permute-start.1 = (bf16[128,256]{1,0:T(8,128)(2,1)S(1)}, bf16[128,256]{1,0:T(8,128)(2,1)S(1)}, u32[]{:S(2)}, u32[]{:S(2)}) collective-permute-start(bf16[128,256]{1,0:T(8,128)(2,1)S(1)} %pad_maximum_fusion.1), channel_id=1, source_target_pairs={{0,8},{2,10},{4,12},{6,14},{8,0},{10,2},{12,4},{14,6},{16,24},{18,... | collective-permute-start | bytes 196616 | tf_op jit(solution)/shard_map/ppermute | solution.py:214
  14.3 2.7 %collective-permute-done.1 = bf16[128,256]{1,0:T(8,128)(2,1)S(1)} collective-permute-done((bf16[128,256]{1,0:T(8,128)(2,1)S(1)}, bf16[128,256]{1,0:T(8,128)(2,1)S(1)}, u32[]{:S(2)}, u32[]{:S(2)}) %collective-permute-start.1) | collective-permute-done | bytes 65568 | tf_op jit(solution)/shard_map/ppermute | solution.py:214
  17.0 2.7 %collective-permute-start.2 = (bf16[256,256]{1,0:T(8,128)(2,1)S(1)}, bf16[256,256]{1,0:T(8,128)(2,1)S(1)}, u32[]{:S(2)}, u32[]{:S(2)}) collective-permute-start(bf16[256,256]{1,0:T(8,128)(2,1)S(1)} %pad_maximum_fusion), channel_id=1, source_target_pairs={{0,16},{2,18},{4,20},{6,22},{8,24},{10,26},{12,28},{14,30},{16,0},... | collective-permute-start | bytes 393224 | tf_op jit(solution)/shard_map/ppermute | solution.py:214
  19.7 4.9 %collective-permute-done.2 = bf16[256,256]{1,0:T(8,128)(2,1)S(1)} collective-permute-done((bf16[256,256]{1,0:T(8,128)(2,1)S(1)}, bf16[256,256]{1,0:T(8,128)(2,1)S(1)}, u32[]{:S(2)}, u32[]{:S(2)}) %collective-permute-start.2) | collective-permute-done | bytes 131104 | tf_op jit(solution)/shard_map/ppermute | solution.py:214
  24.6 0.1 collective-permute-start.3
  24.7 1.2 %convolution_convert_fusion.1.values = bf16[384,128]{1,0:T(8,128)(2,1)} fusion(bf16[384,2048]{1,0:T(8,128)(2,1)S(1)} %copy-done, bf16[2048,128]{1,0:T(8,128)(2,1)S(1)} %copy-done.4), kind=kOutput, calls=%fused_computation.2 | convolution fusion | flops 201375744 | bytes 2195456 | tf_op jit(solution)/shard_map/dot_general | solution.py:222
  25.9 0.3 collective-permute-done.3.far
  26.2 0.7 %copy-done.2 = bf16[512,256]{1,0:T(8,128)(2,1)} copy-done((bf16[512,256]{1,0:T(8,128)(2,1)}, bf16[512,256]{1,0:T(8,128)(2,1)S(1)}, u32[]{:S(2)}) %copy-start.2) | copy-done | bytes 262168
  26.9 6.7 %attend.7 = (bf16[128,1024]{1,0:T(8,128)(2,1)}, bf16[128,1024]{1,0:T(8,128)(2,1)}) custom-call(s32[6,16]{1,0:T(8,128)} %codes.7, s32[16]{0:T(128)} %hot.9, s32[16]{0:T(128)} %get-tuple-element.15.table, f32[16]{0:T(128)} %scale.7, bf16[128,1024]{1,0:T(8,128)(2,1)} %get-tuple-element.25.q, bf16[384,128]{1,0:T(8,128)(2,1)} %convolution_convert_fusion.2.keys, ...), custom_call_target="tpu_custom_call" | custom-call | tf_op jit(solution)/shard_map/attend/pallas_call | solution.py:234
  33.7 1.5 %collective-permute-start.7 = (bf16[128,1024]{1,0:T(8,128)(2,1)}, bf16[128,1024]{1,0:T(8,128)(2,1)S(1)}, u32[]{:S(2)}, u32[]{:S(2)}) collective-permute-start(bf16[128,1024]{1,0:T(8,128)(2,1)} %get-tuple-element.24), channel_id=1, source_target_pairs={{0,1},{1,0},{2,3},{3,2},{4,5},{5,4},{6,7},{7,6},{8,9},{9,8},{10,11... | collective-permute-start | bytes 786440 | tf_op jit(solution)/shard_map/ppermute | solution.py:264
  35.2 6.7 %attend.6 = (bf16[128,1024]{1,0:T(8,128)(2,1)}, bf16[128,1024]{1,0:T(8,128)(2,1)}) custom-call(s32[6,16]{1,0:T(8,128)} %codes.7, s32[16]{0:T(128)} %hot.9, s32[16]{0:T(128)} %get-tuple-element.15.table, f32[16]{0:T(128)} %scale.7, bf16[128,1024]{1,0:T(8,128)(2,1)} %get-tuple-element.26.q, bf16[384,128]{1,0:T(8,128)(2,1)} %convolution_convert_fusion.2.keys, ...), custom_call_target="tpu_custom_call" | custom-call | tf_op jit(solution)/shard_map/attend/pallas_call | solution.py:234
  41.9 0.6 collective-permute-start.6
  42.5 0.7 %fusion.1 = (bf16[64,1024]{1,0:T(8,128)(2,1)}, bf16[64,1024]{1,0:T(8,128)(2,1)}) fusion(bf16[384,1024]{1,0:T(8,128)(2,1)S(1)} %convolution_convert_fusion), kind=kLoop, calls=%fused_computation.11 | loop fusion | bytes 524288 | tf_op jit(solution)/shard_map/slice | solution.py:254
  43.3 5.5 %attend.5 = (bf16[64,1024]{1,0:T(8,128)(2,1)}, bf16[64,1024]{1,0:T(8,128)(2,1)}) custom-call(s32[6,16]{1,0:T(8,128)} %codes.7, s32[16]{0:T(128)} %hot.9, s32[16]{0:T(128)} %get-tuple-element.15.table, f32[16]{0:T(128)} %scale.7, bf16[64,1024]{1,0:T(8,128)(2,1)} %get-tuple-element.27.q, bf16[384,128]{1,0:T(8,128)(2,1)} %convolution_convert_fusion.2.keys, ...), custom_call_target="tpu_custom_call" | custom-call | tf_op jit(solution)/shard_map/attend/pallas_call | solution.py:234
  48.7 1.5 %collective-permute-start.5 = (bf16[64,1024]{1,0:T(8,128)(2,1)}, bf16[64,1024]{1,0:T(8,128)(2,1)S(1)}, u32[]{:S(2)}, u32[]{:S(2)}) collective-permute-start(bf16[64,1024]{1,0:T(8,128)(2,1)} %get-tuple-element.22), channel_id=1, source_target_pairs={{0,1},{1,0},{2,3},{3,2},{4,5},{5,4},{6,7},{7,6},{8,9},{9,8},{10,11... | collective-permute-start | bytes 393224 | tf_op jit(solution)/shard_map/ppermute | solution.py:264
  50.3 5.7 %attend.4 = (bf16[64,1024]{1,0:T(8,128)(2,1)}, bf16[64,1024]{1,0:T(8,128)(2,1)}) custom-call(s32[6,16]{1,0:T(8,128)} %codes.7, s32[16]{0:T(128)} %hot.9, s32[16]{0:T(128)} %get-tuple-element.15.table, f32[16]{0:T(128)} %scale.7, bf16[64,1024]{1,0:T(8,128)(2,1)} %get-tuple-element.28.q, bf16[384,128]{1,0:T(8,128)(2,1)} %convolution_convert_fusion.2.keys, ...), custom_call_target="tpu_custom_call" | custom-call | tf_op jit(solution)/shard_map/attend/pallas_call | solution.py:234
  56.0 0.6 collective-permute-start.4
  56.6 5.1 %own_part.1 = bf16[384,1024]{1,0:T(8,128)(2,1)} custom-call(bf16[64,1024]{1,0:T(8,128)(2,1)} %get-tuple-element.17.refs_0_, bf16[64,1024]{1,0:T(8,128)(2,1)} %get-tuple-element.18.refs_1_, bf16[128,1024]{1,0:T(8,128)(2,1)} %get-tuple-element.19.refs_2_, bf16[128,1024]{1,0:T(8,128)(2,1)} %get-tuple-element.20.refs_3_, bf16[1024,2048]{1,0:T(8,128)(2,1)} %refs_4_.1), custom_call_target="tpu_custom_call" | custom-call | tf_op jit(solution)/shard_map/own_part/pallas_call | solution.py:266
  61.7 2.3 %add_convert_fusion = bf16[384,1024]{1,0:T(8,128)(2,1)} fusion(bf16[384,1024]{1,0:T(8,128)(2,1)} %own_part.1, bf16[128,1024]{1,0:T(8,128)(2,1)S(1)} %collective-permute-done.7, bf16[128,1024]{1,0:T(8,128)(2,1)S(1)} %collective-permute-done.6, bf16[64,1024]{1,0:T(8,128)(2,1)S(1)} %collective-permute-done.5, bf16[64,1024]{1,0:T(8,128)(2,1)S(1)} %collective-permute-done.4), kind=kLoop, calls=%fused_computation | loop fusion | flops 4325376 | bytes 2359296 | tf_op jit(solution)/shard_map/convert_element_type | solution.py:280
  (22 shorter events, 0.1 us)
Async XLA Ops:
  0.0 6.6 %copy-start = (bf16[384,2048]{1,0:T(8,128)(2,1)S(1)}, bf16[384,2048]{1,0:T(8,128)(2,1)}, u32[]{:S(2)}) copy-start(bf16[384,2048]{1,0:T(8,128)(2,1)} %hidden.1) | copy-start | bytes 4718596
  0.0 6.6 %copy-start.3 = (bf16[2048,128]{1,0:T(8,128)(2,1)S(1)}, bf16[2048,128]{1,0:T(8,128)(2,1)}, u32[]{:S(2)}) copy-start(bf16[2048,128]{1,0:T(8,128)(2,1)} %wk.1) | copy-start | bytes 1572868
  3.6 9.1 %collective-permute-start = (bf16[64,256]{1,0:T(8,128)(2,1)}, bf16[64,256]{1,0:T(8,128)(2,1)S(1)}, u32[]{:S(2)}, u32[]{:S(2)}) collective-permute-start(bf16[64,256]{1,0:T(8,128)(2,1)} %get-tuple-element.16), channel_id=1, source_target_pairs={{0,4},{2,6},{4,0},{6,2},{8,12},{10,14},{12,8},{14,10},{16,20},{18,... | collective-permute-start | bytes 98312 | tf_op jit(solution)/shard_map/ppermute | solution.py:214
  7.8 4.8 %copy-start.5 = (bf16[64,256]{1,0:T(8,128)(2,1)S(1)}, bf16[64,256]{1,0:T(8,128)(2,1)}, u32[]{:S(2)}) copy-start(bf16[64,256]{1,0:T(8,128)(2,1)} %get-tuple-element.16) | copy-start | bytes 98308
  11.8 12.9 %copy-start.4 = (bf16[2048,128]{1,0:T(8,128)(2,1)S(1)}, bf16[2048,128]{1,0:T(8,128)(2,1)}, u32[]{:S(2)}) copy-start(bf16[2048,128]{1,0:T(8,128)(2,1)} %wv.1) | copy-start | bytes 1572868
  12.7 4.3 %collective-permute-start.1 = (bf16[128,256]{1,0:T(8,128)(2,1)S(1)}, bf16[128,256]{1,0:T(8,128)(2,1)S(1)}, u32[]{:S(2)}, u32[]{:S(2)}) collective-permute-start(bf16[128,256]{1,0:T(8,128)(2,1)S(1)} %pad_maximum_fusion.1), channel_id=1, source_target_pairs={{0,8},{2,10},{4,12},{6,14},{8,0},{10,2},{12,4},{14,6},{16,24},{18,... | collective-permute-start | bytes 196616 | tf_op jit(solution)/shard_map/ppermute | solution.py:214
  17.0 7.6 %collective-permute-start.2 = (bf16[256,256]{1,0:T(8,128)(2,1)S(1)}, bf16[256,256]{1,0:T(8,128)(2,1)S(1)}, u32[]{:S(2)}, u32[]{:S(2)}) collective-permute-start(bf16[256,256]{1,0:T(8,128)(2,1)S(1)} %pad_maximum_fusion), channel_id=1, source_target_pairs={{0,16},{2,18},{4,20},{6,22},{8,24},{10,26},{12,28},{14,30},{16,0},... | collective-permute-start | bytes 393224 | tf_op jit(solution)/shard_map/ppermute | solution.py:214
  24.6 1.6 %copy-start.1 = (bf16[512,256]{1,0:T(8,128)(2,1)}, bf16[512,256]{1,0:T(8,128)(2,1)S(1)}, u32[]{:S(2)}) copy-start(bf16[512,256]{1,0:T(8,128)(2,1)S(1)} %constant_dynamic-update-slice_fusion.near) | copy-start | bytes 786436
  24.6 1.6 %collective-permute-start.3 = (bf16[512,256]{1,0:T(8,128)(2,1)S(1)}, bf16[512,256]{1,0:T(8,128)(2,1)S(1)}, u32[]{:S(2)}, u32[]{:S(2)}) collective-permute-start(bf16[512,256]{1,0:T(8,128)(2,1)S(1)} %constant_dynamic-update-slice_fusion.near), channel_id=1, source_target_pairs={{0,2},{2,0},{4,6},{6,4},{8,10},{10,8},{12,14},{14,12},{16,18},{18,... | collective-permute-start | bytes 786440 | tf_op jit(solution)/shard_map/ppermute | solution.py:214
  26.2 0.7 %copy-start.2 = (bf16[512,256]{1,0:T(8,128)(2,1)}, bf16[512,256]{1,0:T(8,128)(2,1)S(1)}, u32[]{:S(2)}) copy-start(bf16[512,256]{1,0:T(8,128)(2,1)S(1)} %collective-permute-done.3.far) | copy-start | bytes 786436
  33.7 28.0 %collective-permute-start.7 = (bf16[128,1024]{1,0:T(8,128)(2,1)}, bf16[128,1024]{1,0:T(8,128)(2,1)S(1)}, u32[]{:S(2)}, u32[]{:S(2)}) collective-permute-start(bf16[128,1024]{1,0:T(8,128)(2,1)} %get-tuple-element.24), channel_id=1, source_target_pairs={{0,1},{1,0},{2,3},{3,2},{4,5},{5,4},{6,7},{7,6},{8,9},{9,8},{10,11... | collective-permute-start | bytes 786440 | tf_op jit(solution)/shard_map/ppermute | solution.py:264
  41.9 19.8 %collective-permute-start.6 = (bf16[128,1024]{1,0:T(8,128)(2,1)}, bf16[128,1024]{1,0:T(8,128)(2,1)S(1)}, u32[]{:S(2)}, u32[]{:S(2)}) collective-permute-start(bf16[128,1024]{1,0:T(8,128)(2,1)} %get-tuple-element.23), channel_id=1, source_target_pairs={{0,1},{1,0},{2,3},{3,2},{4,5},{5,4},{6,7},{7,6},{8,9},{9,8},{10,11... | collective-permute-start | bytes 786440 | tf_op jit(solution)/shard_map/ppermute | solution.py:264
  48.7 12.9 %collective-permute-start.5 = (bf16[64,1024]{1,0:T(8,128)(2,1)}, bf16[64,1024]{1,0:T(8,128)(2,1)S(1)}, u32[]{:S(2)}, u32[]{:S(2)}) collective-permute-start(bf16[64,1024]{1,0:T(8,128)(2,1)} %get-tuple-element.22), channel_id=1, source_target_pairs={{0,1},{1,0},{2,3},{3,2},{4,5},{5,4},{6,7},{7,6},{8,9},{9,8},{10,11... | collective-permute-start | bytes 393224 | tf_op jit(solution)/shard_map/ppermute | solution.py:264
  56.0 5.7 %collective-permute-start.4 = (bf16[64,1024]{1,0:T(8,128)(2,1)}, bf16[64,1024]{1,0:T(8,128)(2,1)S(1)}, u32[]{:S(2)}, u32[]{:S(2)}) collective-permute-start(bf16[64,1024]{1,0:T(8,128)(2,1)} %get-tuple-element.21), channel_id=1, source_target_pairs={{0,1},{1,0},{2,3},{3,2},{4,5},{5,4},{6,7},{7,6},{8,9},{9,8},{10,11... | collective-permute-start | bytes 393224 | tf_op jit(solution)/shard_map/ppermute | solution.py:264

commit v2 on v1

v2 whole, which is shorter than its diff:
```python
import functools

import jax
import jax.numpy as jnp
from jax import lax
from jax.experimental import pallas as pl
from jax.experimental.pallas import tpu as pltpu
from jax.sharding import PartitionSpec as P

HD = 64
KB = 32
QB = 64
NSEL = 16
NHOT = 16
HOT_MOST = 2


def exchange_steps(count):
    steps = []
    step = 2
    while step < count:
        steps.append(step)
        step *= 2
    if count > 1:
        steps.append(1)
    return steps


def slot_kernel(hot, hidden, wk, wv, slots, rows, sem, *, own_blocks):
    base = lax.axis_index("kv") * own_blocks
    offs = [jnp.int32(0) for _ in range(HOT_MOST)]
    seen = jnp.int32(0)
    for h in range(NHOT):
        off = hot[h] - base
        mine = (off >= 0) & (off < own_blocks)
        for r in range(HOT_MOST):
            offs[r] = jnp.where(mine & (seen == r), off, offs[r])
        seen = seen + jnp.where(mine, 1, 0)
    copies = []
    for r in range(HOT_MOST):
        copy = pltpu.make_async_copy(
            hidden.at[pl.ds(pl.multiple_of(offs[r] * KB, KB), KB)],
            rows.at[pl.ds(r * KB, KB)],
            sem.at[r],
        )
        copy.start()
        copies.append(copy)
    for copy in copies:
        copy.wait()
    x = rows[...]
    half = wk.shape[1]
    slots[:, :half] = jnp.dot(x, wk[...], preferred_element_type=jnp.float32).astype(jnp.bfloat16)
    slots[:, half:] = jnp.dot(x, wv[...], preferred_element_type=jnp.float32).astype(jnp.bfloat16)


def table_kernel(hot, table, *, own_blocks, steps):
    me = lax.axis_index("kv")
    owners = [lax.div(hot[h], own_blocks) for h in range(NHOT)]
    for h in range(NHOT):
        rank = jnp.int32(0)
        for g in range(h):
            rank = rank + jnp.where(owners[g] == owners[h], 1, 0)
        apart = owners[h] ^ me
        place = jnp.int32(0)
        for j, step in enumerate(steps):
            place = place + jnp.where((apart & step) != 0, 1 << j, 0)
        table[h] = (own_blocks + place * HOT_MOST + rank) * KB


def attend_kernel(
    codes,
    hot,
    table,
    scale,
    q,
    keys,
    values,
    near,
    far,
    *rest,
    first,
    count,
):
    att, pool, picked, s_buf, p_buf = rest[-5:]
    me = lax.axis_index("kv")
    tok_rows, kw = keys.shape
    own_blocks = tok_rows // KB
    kv_heads = kw // HD
    group = q.shape[1] // HD // kv_heads
    near_rows = near.shape[0]
    pool[:tok_rows, :kw] = keys[...]
    pool[:tok_rows, kw:] = values[...]
    pool[tok_rows : tok_rows + near_rows, :] = near[...]
    pool[tok_rows + near_rows :, :] = far[...]
    lane = lax.broadcasted_iota(jnp.int32, (1, NSEL * KB), 1)
    lane_block = lane // KB
    for b in range(count):
        key_pos = lane - lane_block * KB
        for e in range(NSEL):
            code = codes[first + b, e]
            hot_at = jnp.maximum(code - own_blocks, 0)
            is_own = code < own_blocks
            row = jnp.where(is_own, code * KB, table[hot_at])
            block = jnp.where(is_own, me * own_blocks + code, hot[hot_at])
            key_pos = key_pos + jnp.where(lane_block == e, block * KB, 0)
            picked[e * KB : (e + 1) * KB, :] = pool[pl.ds(pl.multiple_of(row, KB), KB), :]
        query_pos = (
            me * tok_rows + (first + b) * QB + lax.broadcasted_iota(jnp.int32, (QB, 1), 0)
        )
        bias = jnp.where(key_pos <= query_pos, 0.0, -jnp.inf).astype(jnp.float32)
        for c in range(kv_heads):
            heads = [c * group + g for g in range(group)]
            q_rows = jnp.concatenate(
                [q[b * QB : (b + 1) * QB, h * HD : (h + 1) * HD] for h in heads], axis=0
            )
            s_buf[...] = lax.dot_general(
                q_rows,
                picked[:, c * HD : (c + 1) * HD],
                (((1,), (1,)), ((), ())),
                preferred_element_type=jnp.float32,
            )
            sums = []
            for g, h in enumerate(heads):
                at = slice(g * QB, (g + 1) * QB)
                s = s_buf[at, :] * (scale[h] * HD ** (-0.5)) + bias
                lifted = jnp.exp(s - jnp.max(s, axis=-1, keepdims=True))
                sums.append(jnp.sum(lifted, axis=-1, keepdims=True))
                p_buf[at, :] = lifted.astype(jnp.bfloat16)
            out = jnp.dot(
                p_buf[...],
                picked[:, kw + c * HD : kw + (c + 1) * HD],
                preferred_element_type=jnp.float32,
            )
            for g, h in enumerate(heads):
                att[b * QB : (b + 1) * QB, h * HD : (h + 1) * HD] = (
                    out[g * QB : (g + 1) * QB, :] / sums[g]
                ).astype(jnp.bfloat16)


def local(
    hidden_rows,
    proj_query,
    proj_key,
    proj_value,
    proj_output,
    head_scale,
    hot_blocks,
    chosen_blocks,
    *,
    n_kv,
    n_tp,
):
    tok_rows = hidden_rows.shape[0]
    own_blocks = tok_rows // KB
    kw = proj_key.shape[1]
    width = 2 * kw
    heads_w = proj_query.shape[1]
    part = proj_output.shape[1] // n_tp
    query_blocks = tok_rows // QB
    steps = exchange_steps(n_kv)
    smem = pl.BlockSpec(memory_space=pltpu.SMEM)
    vmem = pl.BlockSpec(memory_space=pltpu.VMEM)
    anym = pl.BlockSpec(memory_space=pl.ANY)
    slot_rows = HOT_MOST * KB
    slots = pl.pallas_call(
        functools.partial(slot_kernel, own_blocks=own_blocks),
        out_shape=jax.ShapeDtypeStruct((slot_rows, width), jnp.bfloat16),
        in_specs=[smem, anym, vmem, vmem],
        out_specs=vmem,
        scratch_shapes=[
            pltpu.VMEM((slot_rows, hidden_rows.shape[1]), jnp.bfloat16),
            pltpu.SemaphoreType.DMA((HOT_MOST,)),
        ],
        name="slot_rows",
    )(hot_blocks, hidden_rows, proj_key, proj_value)
    table = pl.pallas_call(
        functools.partial(table_kernel, own_blocks=own_blocks, steps=steps),
        out_shape=jax.ShapeDtypeStruct((NHOT,), jnp.int32),
        in_specs=[smem],
        out_specs=smem,
        name="table",
    )(hot_blocks)

    def swap(x, step):
        return lax.ppermute(x, "kv", [(i, i ^ step) for i in range(n_kv)])

    def project(w):
        return jnp.dot(hidden_rows, w, preferred_element_type=jnp.float32).astype(jnp.bfloat16)

    here = lax.axis_index("tp")
    wo_parts = [
        lax.dynamic_slice_in_dim(proj_output, lax.rem(here + d, n_tp) * part, part, axis=1)
        for d in range(n_tp)
    ]
    queries = project(proj_query)
    keys = project(proj_key)
    values = project(proj_value)
    near = slots
    for step in steps[:-1]:
        near = jnp.concatenate([near, swap(near, step)], axis=0)
    near, table, keys, values, queries, *wo_parts = lax.optimization_barrier(
        (near, table, keys, values, queries, *wo_parts)
    )
    far = swap(near, steps[-1])
    per = 2 if query_blocks % 2 == 0 else 1
    rows = per * QB
    atts, pieces, sent = [], [], []
    group_rows = heads_w // HD // (kw // HD) * QB
    for chunk in range(query_blocks // per):
        att = pl.pallas_call(
            functools.partial(attend_kernel, first=chunk * per, count=per),
            out_shape=jax.ShapeDtypeStruct((rows, heads_w), jnp.bfloat16),
            grid=(1,),
            in_specs=[
                smem,
                smem,
                smem,
                smem,
                pl.BlockSpec((rows, heads_w), lambda i, chunk=chunk: (chunk, 0)),
                vmem,
                vmem,
                vmem,
                vmem,
            ]
            + [anym] * len(sent),
            out_specs=pl.BlockSpec((rows, heads_w), lambda i: (0, 0)),
            scratch_shapes=[
                pltpu.VMEM((tok_rows + near.shape[0] + far.shape[0], width), jnp.bfloat16),
                pltpu.VMEM((NSEL * KB, width), jnp.bfloat16),
                pltpu.VMEM((group_rows, NSEL * KB), jnp.float32),
                pltpu.VMEM((group_rows, NSEL * KB), jnp.bfloat16),
            ],
            name="attend",
        )(chosen_blocks, hot_blocks, table, head_scale, queries, keys, values, near, far, *sent)
        atts.append(att)
        got, sends = [], []
        for d in range(1, n_tp):
            send = jnp.dot(att, wo_parts[d], preferred_element_type=jnp.float32).astype(
                jnp.bfloat16
            )
            pairs = [(i, (i + d) % n_tp) for i in range(n_tp)]
            got.append(lax.ppermute(send, "tp", pairs))
            sends.append(send)
        sent = sends
        pieces.append(got)

    def total(own, got):
        out = own.astype(jnp.float32)
        for piece in got:
            out = out + piece.astype(jnp.float32)
        return out.astype(jnp.bfloat16)

    own = [
        jnp.dot(att, wo_parts[0], preferred_element_type=jnp.float32).astype(jnp.bfloat16)
        for att in atts
    ]
    sums = [total(o, g) for o, g in zip(own[:-1], pieces[:-1])]
    out = jnp.concatenate(sums + [own[-1]], axis=0)
    out, last = lax.optimization_barrier((out, own[-1]))
    return lax.dynamic_update_slice(out, total(last, pieces[-1]), (tok_rows - rows, 0))


def solution(mesh):
    return jax.shard_map(
        functools.partial(local, n_kv=mesh.shape["kv"], n_tp=mesh.shape["tp"]),
        mesh=mesh,
        in_specs=(
            P("kv", None),
            P(None, "tp"),
            P(None, "tp"),
            P(None, "tp"),
            P("tp", None),
            P("tp"),
            P(),
            P("kv", None),
        ),
        out_specs=P("kv", "tp"),
        check_vma=False,
    )
```

time: 64.5 us -> 57.1 us (0.89)
  Pallas kernels: 33.2 us -> 18.3 us
  matrix products: 6.41 us -> 13 us
  local copies, waits for them, and re-layouts: 2.27 us -> 5.19 us
  waiting for transfers between devices: 7.91 us -> 7.21 us
    pallas_call x6 -> x5, Pallas kernels: 33.2 us -> 18.3 us  [the longest x3 13.6 us: local(): pl.pallas_call(functools.partial(attend_kernel, first=chunk * per, count=...]
    dot_general x0 -> x6, matrix products: none -> 5.67 us  [the longest x3 4.33 us: local(): jnp.dot(att, wo_parts[d], preferred_element_type=jnp.float32)]
    ppermute x4, waiting for transfers between devices: 7.9 us -> 3.33 us  [swap(): return lax.ppermute(x, 'kv', [(i, i ^ step) for i in range(n_kv)])]
    dynamic_slice x0 -> x1, local copies, waits for them, and re-layouts: none -> 4 us  [local(): lax.dynamic_slice_in_dim(proj_output, lax.rem(here + d, n_tp) * part, par...]
    ppermute x4 -> x3, waiting for transfers between devices: 0.01 us -> 3.88 us  [local(): got.append(lax.ppermute(send, 'tp', pairs))]
    convert_element_type x1 -> x0, other arithmetic: 2.32 us -> none  [local(): return total.astype(jnp.bfloat16)]
    slice x2 -> x0, local copies, waits for them, and re-layouts: 1.53 us -> none  [local(): queries[first * QB:first * QB + rows]]
    concatenate x0 -> x1, other arithmetic: none -> 0.93 us  [local(): out = jnp.concatenate(sums + [own[-1]], axis=0)]
  transfers between devices with their start and end apart: 8 -> 7, of which waited for: 3 -> 3; matrix products, arithmetic and copies ran while one was open for 12% -> 29% of each run, Pallas kernels for 36% -> 19%
where the time goes in v2:
time: 57.1 us; the launch traced here: 56.7 us
  Pallas kernels  18.3 us (32%)
  matrix products  13 us (23%)
  starting transfers between devices  11.1 us (19%)
  waiting for transfers between devices  7.21 us (13%)
  local copies, waits for them, and re-layouts  5.19 us (9%)
  other arithmetic  1.74 us (3%)
    pallas_call x3, Pallas kernels, local(): pl.pallas_call(functools.partial(attend_kernel, first=chunk * per, count=...  13.6 us
    ppermute x4, starting transfers between devices, swap(): return lax.ppermute(x, 'kv', [(i, i ^ step) for i in range(n_kv)])  7.43 us
    dot_general x3, matrix products, project(): jnp.dot(hidden_rows, w, preferred_element_type=jnp.float32)  7.29 us
    dot_general x3, matrix products, local(): jnp.dot(att, wo_parts[d], preferred_element_type=jnp.float32)  4.33 us
    dynamic_slice x1, local copies, waits for them, and re-layouts, local(): lax.dynamic_slice_in_dim(proj_output, lax.rem(here + d, n_tp) * part, par...  4 us
    ppermute x3, waiting for transfers between devices, local(): got.append(lax.ppermute(send, 'tp', pairs))  3.88 us
    ppermute x3, starting transfers between devices, local(): got.append(lax.ppermute(send, 'tp', pairs))  3.72 us
    ppermute x4, waiting for transfers between devices, swap(): return lax.ppermute(x, 'kv', [(i, i ^ step) for i in range(n_kv)])  3.33 us
  transfers between devices with their start and end apart: 7, of which 3 were waited for; matrix products, arithmetic and copies ran while one was open for 29% of the time, Pallas kernels for 19%

profile of v2, /device:TPU:0, one launch (start us, length us, event | category | flops | bytes accessed | tf_op | source)
XLA Modules:
  0.0 56.7 jit_solution(991440335572222928)
XLA Ops:
  0.0 3.3 %slot_rows.1 = bf16[64,256]{1,0:T(8,128)(2,1)} custom-call(s32[16]{0:T(128)} %hot.9, bf16[384,2048]{1,0:T(8,128)(2,1)} %hidden.1, bf16[2048,128]{1,0:T(8,128)(2,1)} %wk.1, bf16[2048,128]{1,0:T(8,128)(2,1)} %wv.1), custom_call_target="tpu_custom_call" | custom-call | tf_op jit(solution)/shard_map/slot_rows/pallas_call | solution.py:165
  3.3 3.1 %collective-permute-start = (bf16[64,256]{1,0:T(8,128)(2,1)}, bf16[64,256]{1,0:T(8,128)(2,1)S(1)}, u32[]{:S(2)}, u32[]{:S(2)}) collective-permute-start(bf16[64,256]{1,0:T(8,128)(2,1)} %slot_rows.1), channel_id=1, source_target_pairs={{0,4},{2,6},{4,0},{6,2},{8,12},{10,14},{12,8},{14,10},{16,20},{18,... | collective-permute-start | bytes 98312 | tf_op jit(solution)/shard_map/ppermute | solution.py:185
  6.4 4.9 %convolution_convert_fusion.q = bf16[384,1024]{1,0:T(8,128)(2,1)} fusion(bf16[384,2048]{1,0:T(8,128)(2,1)S(1)} %copy-done.1, bf16[2048,1024]{1,0:T(8,128)(2,1)} %param.9), kind=kOutput, calls=%fused_computation | convolution fusion | flops 1611005952 | bytes 6553600 | tf_op jit(solution)/shard_map/dot_general | solution.py:188
  11.2 1.2 %convolution_convert_fusion.8.keys = bf16[384,128]{1,0:T(8,128)(2,1)} fusion(bf16[384,2048]{1,0:T(8,128)(2,1)S(1)} %copy-done.1, bf16[2048,128]{1,0:T(8,128)(2,1)S(1)} %copy-done.7), kind=kOutput, calls=%fused_computation.14 | convolution fusion | flops 201375744 | bytes 2195456 | tf_op jit(solution)/shard_map/dot_general | solution.py:188
  12.5 1.6 %collective-permute-start.1 = (bf16[128,256]{1,0:T(8,128)(2,1)S(1)}, bf16[128,256]{1,0:T(8,128)(2,1)S(1)}, u32[]{:S(2)}, u32[]{:S(2)}) collective-permute-start(bf16[128,256]{1,0:T(8,128)(2,1)S(1)} %pad_maximum_fusion.3), channel_id=1, source_target_pairs={{0,8},{2,10},{4,12},{6,14},{8,0},{10,2},{12,4},{14,6},{16,24},{18,... | collective-permute-start | bytes 196616 | tf_op jit(solution)/shard_map/ppermute | solution.py:185
  14.1 1.2 %convolution_convert_fusion.7.values = bf16[384,128]{1,0:T(8,128)(2,1)} fusion(bf16[384,2048]{1,0:T(8,128)(2,1)S(1)} %copy-done.1, bf16[2048,128]{1,0:T(8,128)(2,1)S(1)} %copy-done.8), kind=kOutput, calls=%fused_computation.13 | convolution fusion | flops 201375744 | bytes 2195456 | tf_op jit(solution)/shard_map/dot_general | solution.py:188
  15.3 1.4 %table.1 = s32[16]{0:T(128)} custom-call(s32[16]{0:T(128)} %hot.9), custom_call_target="tpu_custom_call" | custom-call | tf_op jit(solution)/shard_map/table/pallas_call | solution.py:176
  16.8 2.7 %collective-permute-start.2 = (bf16[256,256]{1,0:T(8,128)(2,1)S(1)}, bf16[256,256]{1,0:T(8,128)(2,1)S(1)}, u32[]{:S(2)}, u32[]{:S(2)}) collective-permute-start(bf16[256,256]{1,0:T(8,128)(2,1)S(1)} %pad_maximum_fusion.2), channel_id=1, source_target_pairs={{0,16},{2,18},{4,20},{6,22},{8,24},{10,26},{12,28},{14,30},{16,0},... | collective-permute-start | bytes 393224 | tf_op jit(solution)/shard_map/ppermute | solution.py:185
  19.5 4.0 %constant_dynamic-slice_fusion = (bf16[1024,1024]{1,0:T(8,128)(2,1)S(1)}, bf16[1024,1024]{1,0:T(8,128)(2,1)}) fusion(bf16[1024,2048]{1,0:T(8,128)(2,1)} %param.12, s32[]{:T(128)S(6)} %select_n.7, s32[]{:T(128)S(6)} %select_n.6), kind=kLoop, calls=%fused_computation.21 | loop fusion | bytes 8388616 | tf_op jit(solution)/shard_map/dynamic_slice | solution.py:192
  23.5 1.8 %collective-permute-done.2 = bf16[256,256]{1,0:T(8,128)(2,1)S(1)} collective-permute-done((bf16[256,256]{1,0:T(8,128)(2,1)S(1)}, bf16[256,256]{1,0:T(8,128)(2,1)S(1)}, u32[]{:S(2)}, u32[]{:S(2)}) %collective-permute-start.2) | collective-permute-done | bytes 131104 | tf_op jit(solution)/shard_map/ppermute | solution.py:185
  25.4 1.5 %collective-permute-done.3.far = bf16[512,256]{1,0:T(8,128)(2,1)S(1)} collective-permute-done((bf16[512,256]{1,0:T(8,128)(2,1)S(1)}, bf16[512,256]{1,0:T(8,128)(2,1)S(1)}, u32[]{:S(2)}, u32[]{:S(2)}) %collective-permute-start.3) | collective-permute-done | bytes 262176 | tf_op jit(solution)/shard_map/ppermute | solution.py:185
  26.9 0.7 %copy-done.6 = bf16[512,256]{1,0:T(8,128)(2,1)} copy-done((bf16[512,256]{1,0:T(8,128)(2,1)}, bf16[512,256]{1,0:T(8,128)(2,1)S(1)}, u32[]{:S(2)}) %copy-start.6) | copy-done | bytes 262168
  27.6 4.5 %attend.3 = bf16[128,1024]{1,0:T(8,128)(2,1)} custom-call(s32[6,16]{1,0:T(8,128)} %codes.5, s32[16]{0:T(128)} %hot.9, s32[16]{0:T(128)} %table.1, f32[16]{0:T(128)} %scale.5, bf16[384,1024]{1,0:T(8,128)(2,1)} %convolution_convert_fusion.q, bf16[384,128]{1,0:T(8,128)(2,1)} %convolution_convert_fusion.8.keys, ...), custom_call_target="tpu_custom_call" | custom-call | tf_op jit(solution)/shard_map/attend/pallas_call | solution.py:210
  32.1 1.4 %convolution_convert_fusion.5.rest_0_ = bf16[128,1024]{1,0:T(8,128)(2,1)S(1)} fusion(bf16[128,1024]{1,0:T(8,128)(2,1)} %attend.3, bf16[1024,1024]{1,0:T(8,128)(2,1)S(1)} %get-tuple-element.20), kind=kOutput, calls=%fused_computation.7 | convolution fusion | flops 268566528 | bytes 2621440 | tf_op jit(solution)/shard_map/dot_general | solution.py:238
  33.5 1.6 %collective-permute-start.4 = (bf16[128,1024]{1,0:T(8,128)(2,1)S(1)}, bf16[128,1024]{1,0:T(8,128)(2,1)S(1)}, u32[]{:S(2)}, u32[]{:S(2)}) collective-permute-start(bf16[128,1024]{1,0:T(8,128)(2,1)S(1)} %convolution_convert_fusion.5.rest_0_), channel_id=1, source_target_pairs={{0,1},{1,0},{2,3},{3,2},{4,5},{5,4},{6,7},{7,6},{8,9},{9,8},{10,11... | collective-permute-start | bytes 786440 | tf_op jit(solution)/shard_map/ppermute | solution.py:242
  35.1 4.5 %attend.4 = bf16[128,1024]{1,0:T(8,128)(2,1)} custom-call(s32[6,16]{1,0:T(8,128)} %codes.5, s32[16]{0:T(128)} %hot.9, s32[16]{0:T(128)} %table.1, f32[16]{0:T(128)} %scale.5, bf16[384,1024]{1,0:T(8,128)(2,1)} %convolution_convert_fusion.q, bf16[384,128]{1,0:T(8,128)(2,1)} %convolution_convert_fusion.8.keys, ...), custom_call_target="tpu_custom_call" | custom-call | tf_op jit(solution)/shard_map/attend/pallas_call | solution.py:210
  39.6 1.4 %convolution_convert_fusion.3.rest_0_ = bf16[128,1024]{1,0:T(8,128)(2,1)S(1)} fusion(bf16[128,1024]{1,0:T(8,128)(2,1)} %attend.4, bf16[1024,1024]{1,0:T(8,128)(2,1)S(1)} %get-tuple-element.20), kind=kOutput, calls=%fused_computation.3 | convolution fusion | flops 268566528 | bytes 2621440 | tf_op jit(solution)/shard_map/dot_general | solution.py:238
  41.0 0.7 %collective-permute-start.5 = (bf16[128,1024]{1,0:T(8,128)(2,1)S(1)}, bf16[128,1024]{1,0:T(8,128)(2,1)S(1)}, u32[]{:S(2)}, u32[]{:S(2)}) collective-permute-start(bf16[128,1024]{1,0:T(8,128)(2,1)S(1)} %convolution_convert_fusion.3.rest_0_), channel_id=1, source_target_pairs={{0,1},{1,0},{2,3},{3,2},{4,5},{5,4},{6,7},{7,6},{8,9},{9,8},{10,11... | collective-permute-start | bytes 786440 | tf_op jit(solution)/shard_map/ppermute | solution.py:242
  41.7 4.5 %attend.5 = bf16[128,1024]{1,0:T(8,128)(2,1)} custom-call(s32[6,16]{1,0:T(8,128)} %codes.5, s32[16]{0:T(128)} %hot.9, s32[16]{0:T(128)} %table.1, f32[16]{0:T(128)} %scale.5, bf16[384,1024]{1,0:T(8,128)(2,1)} %convolution_convert_fusion.q, bf16[384,128]{1,0:T(8,128)(2,1)} %convolution_convert_fusion.8.keys, ...), custom_call_target="tpu_custom_call" | custom-call | tf_op jit(solution)/shard_map/attend/pallas_call | solution.py:210
  46.3 1.5 %convolution_convert_fusion.1 = bf16[128,1024]{1,0:T(8,128)(2,1)S(1)} fusion(bf16[128,1024]{1,0:T(8,128)(2,1)} %attend.5, bf16[1024,1024]{1,0:T(8,128)(2,1)S(1)} %get-tuple-element.20), kind=kOutput, calls=%fused_computation.1 | convolution fusion | flops 268566528 | bytes 2621440 | tf_op jit(solution)/shard_map/dot_general | solution.py:238
  47.8 1.5 %collective-permute-start.6 = (bf16[128,1024]{1,0:T(8,128)(2,1)S(1)}, bf16[128,1024]{1,0:T(8,128)(2,1)S(1)}, u32[]{:S(2)}, u32[]{:S(2)}) collective-permute-start(bf16[128,1024]{1,0:T(8,128)(2,1)S(1)} %convolution_convert_fusion.1), channel_id=1, source_target_pairs={{0,1},{1,0},{2,3},{3,2},{4,5},{5,4},{6,7},{7,6},{8,9},{9,8},{10,11... | collective-permute-start | bytes 786440 | tf_op jit(solution)/shard_map/ppermute | solution.py:242
  51.2 0.9 %pad_maximum_fusion = bf16[384,1024]{1,0:T(8,128)(2,1)} fusion(bf16[128,1024]{1,0:T(8,128)(2,1)S(1)} %convolution_convert_fusion.2, bf16[128,1024]{1,0:T(8,128)(2,1)S(1)} %fusion.5, bf16[128,1024]{1,0:T(8,128)(2,1)S(1)} %fusion.4), kind=kLoop, calls=%fused_computation.15 | loop fusion | flops 2359296 | bytes 1572864 | tf_op jit(solution)/shard_map/concatenate | solution.py:258
  52.1 3.9 %collective-permute-done.6 = bf16[128,1024]{1,0:T(8,128)(2,1)S(1)} collective-permute-done((bf16[128,1024]{1,0:T(8,128)(2,1)S(1)}, bf16[128,1024]{1,0:T(8,128)(2,1)S(1)}, u32[]{:S(2)}, u32[]{:S(2)}) %collective-permute-start.6) | collective-permute-done | bytes 262176 | tf_op jit(solution)/shard_map/ppermute | solution.py:242
  56.0 0.8 %fusion.6 = bf16[384,1024]{1,0:T(8,128)(2,1)} fusion(bf16[384,1024]{1,0:T(8,128)(2,1)} %pad_maximum_fusion, bf16[128,1024]{1,0:T(8,128)(2,1)S(1)} %collective-permute-done.6, bf16[128,1024]{1,0:T(8,128)(2,1)S(1)} %convolution_convert_fusion.2), kind=kLoop, calls=%fused_computation.17 | loop fusion | flops 524288 | bytes 786432 | tf_op jit(solution)/shard_map/dynamic_update_slice | solution.py:260
  (34 shorter events, 2.0 us)
Async XLA Ops:
  0.0 6.4 %copy-start.1 = (bf16[384,2048]{1,0:T(8,128)(2,1)S(1)}, bf16[384,2048]{1,0:T(8,128)(2,1)}, u32[]{:S(2)}) copy-start(bf16[384,2048]{1,0:T(8,128)(2,1)} %hidden.1) | copy-start | bytes 4718596
  3.3 7.9 %copy-start.7 = (bf16[2048,128]{1,0:T(8,128)(2,1)S(1)}, bf16[2048,128]{1,0:T(8,128)(2,1)}, u32[]{:S(2)}) copy-start(bf16[2048,128]{1,0:T(8,128)(2,1)} %wk.1) | copy-start | bytes 1572868
  3.3 9.1 %collective-permute-start = (bf16[64,256]{1,0:T(8,128)(2,1)}, bf16[64,256]{1,0:T(8,128)(2,1)S(1)}, u32[]{:S(2)}, u32[]{:S(2)}) collective-permute-start(bf16[64,256]{1,0:T(8,128)(2,1)} %slot_rows.1), channel_id=1, source_target_pairs={{0,4},{2,6},{4,0},{6,2},{8,12},{10,14},{12,8},{14,10},{16,20},{18,... | collective-permute-start | bytes 98312 | tf_op jit(solution)/shard_map/ppermute | solution.py:185
  11.2 1.2 %copy-start.11 = (bf16[64,256]{1,0:T(8,128)(2,1)S(1)}, bf16[64,256]{1,0:T(8,128)(2,1)}, u32[]{:S(2)}) copy-start(bf16[64,256]{1,0:T(8,128)(2,1)} %slot_rows.1) | copy-start | bytes 98308
  11.2 2.9 %copy-start.8 = (bf16[2048,128]{1,0:T(8,128)(2,1)S(1)}, bf16[2048,128]{1,0:T(8,128)(2,1)}, u32[]{:S(2)}) copy-start(bf16[2048,128]{1,0:T(8,128)(2,1)} %wv.1) | copy-start | bytes 1572868
  12.5 4.3 %collective-permute-start.1 = (bf16[128,256]{1,0:T(8,128)(2,1)S(1)}, bf16[128,256]{1,0:T(8,128)(2,1)S(1)}, u32[]{:S(2)}, u32[]{:S(2)}) collective-permute-start(bf16[128,256]{1,0:T(8,128)(2,1)S(1)} %pad_maximum_fusion.3), channel_id=1, source_target_pairs={{0,8},{2,10},{4,12},{6,14},{8,0},{10,2},{12,4},{14,6},{16,24},{18,... | collective-permute-start | bytes 196616 | tf_op jit(solution)/shard_map/ppermute | solution.py:185
  16.8 8.5 %collective-permute-start.2 = (bf16[256,256]{1,0:T(8,128)(2,1)S(1)}, bf16[256,256]{1,0:T(8,128)(2,1)S(1)}, u32[]{:S(2)}, u32[]{:S(2)}) collective-permute-start(bf16[256,256]{1,0:T(8,128)(2,1)S(1)} %pad_maximum_fusion.2), channel_id=1, source_target_pairs={{0,16},{2,18},{4,20},{6,22},{8,24},{10,26},{12,28},{14,30},{16,0},... | collective-permute-start | bytes 393224 | tf_op jit(solution)/shard_map/ppermute | solution.py:185
  25.3 1.6 %copy-start.2 = (bf16[512,256]{1,0:T(8,128)(2,1)}, bf16[512,256]{1,0:T(8,128)(2,1)S(1)}, u32[]{:S(2)}) copy-start(bf16[512,256]{1,0:T(8,128)(2,1)S(1)} %pad_maximum_fusion.1.near) | copy-start | bytes 786436
  25.3 1.6 %collective-permute-start.3 = (bf16[512,256]{1,0:T(8,128)(2,1)S(1)}, bf16[512,256]{1,0:T(8,128)(2,1)S(1)}, u32[]{:S(2)}, u32[]{:S(2)}) collective-permute-start(bf16[512,256]{1,0:T(8,128)(2,1)S(1)} %pad_maximum_fusion.1.near), channel_id=1, source_target_pairs={{0,2},{2,0},{4,6},{6,4},{8,10},{10,8},{12,14},{14,12},{16,18},{18,... | collective-permute-start | bytes 786440 | tf_op jit(solution)/shard_map/ppermute | solution.py:185
  26.9 0.7 %copy-start.6 = (bf16[512,256]{1,0:T(8,128)(2,1)}, bf16[512,256]{1,0:T(8,128)(2,1)S(1)}, u32[]{:S(2)}) copy-start(bf16[512,256]{1,0:T(8,128)(2,1)S(1)} %collective-permute-done.3.far) | copy-start | bytes 786436
  33.5 1.6 %copy-start.9 = (bf16[128,1024]{1,0:T(8,128)(2,1)}, bf16[128,1024]{1,0:T(8,128)(2,1)S(1)}, u32[]{:S(2)}) copy-start(bf16[128,1024]{1,0:T(8,128)(2,1)S(1)} %convolution_convert_fusion.5.rest_0_) | copy-start | bytes 786436
  33.5 16.7 %collective-permute-start.4 = (bf16[128,1024]{1,0:T(8,128)(2,1)S(1)}, bf16[128,1024]{1,0:T(8,128)(2,1)S(1)}, u32[]{:S(2)}, u32[]{:S(2)}) collective-permute-start(bf16[128,1024]{1,0:T(8,128)(2,1)S(1)} %convolution_convert_fusion.5.rest_0_), channel_id=1, source_target_pairs={{0,1},{1,0},{2,3},{3,2},{4,5},{5,4},{6,7},{7,6},{8,9},{9,8},{10,11... | collective-permute-start | bytes 786440 | tf_op jit(solution)/shard_map/ppermute | solution.py:242
  41.0 0.7 %copy-start.10 = (bf16[128,1024]{1,0:T(8,128)(2,1)}, bf16[128,1024]{1,0:T(8,128)(2,1)S(1)}, u32[]{:S(2)}) copy-start(bf16[128,1024]{1,0:T(8,128)(2,1)S(1)} %convolution_convert_fusion.3.rest_0_) | copy-start | bytes 786436
  41.0 8.7 %collective-permute-start.5 = (bf16[128,1024]{1,0:T(8,128)(2,1)S(1)}, bf16[128,1024]{1,0:T(8,128)(2,1)S(1)}, u32[]{:S(2)}, u32[]{:S(2)}) collective-permute-start(bf16[128,1024]{1,0:T(8,128)(2,1)S(1)} %convolution_convert_fusion.3.rest_0_), channel_id=1, source_target_pairs={{0,1},{1,0},{2,3},{3,2},{4,5},{5,4},{6,7},{7,6},{8,9},{9,8},{10,11... | collective-permute-start | bytes 786440 | tf_op jit(solution)/shard_map/ppermute | solution.py:242
  46.2 3.1 %copy-start = (bf16[1024,1024]{1,0:T(8,128)(2,1)S(1)}, bf16[1024,1024]{1,0:T(8,128)(2,1)}, u32[]{:S(2)}) copy-start(bf16[1024,1024]{1,0:T(8,128)(2,1)} %get-tuple-element.19) | copy-start | bytes 6291460
  46.2 3.1 %copy-start.4 = (bf16[128,1024]{1,0:T(8,128)(2,1)S(1)}, bf16[128,1024]{1,0:T(8,128)(2,1)}, u32[]{:S(2)}) copy-start(bf16[128,1024]{1,0:T(8,128)(2,1)} %attend.5) | copy-start | bytes 786436
  46.2 3.5 %copy-start.5 = (bf16[128,1024]{1,0:T(8,128)(2,1)S(1)}, bf16[128,1024]{1,0:T(8,128)(2,1)}, u32[]{:S(2)}) copy-start(bf16[128,1024]{1,0:T(8,128)(2,1)} %attend.4) | copy-start | bytes 786436
  47.8 8.2 %collective-permute-start.6 = (bf16[128,1024]{1,0:T(8,128)(2,1)S(1)}, bf16[128,1024]{1,0:T(8,128)(2,1)S(1)}, u32[]{:S(2)}, u32[]{:S(2)}) collective-permute-start(bf16[128,1024]{1,0:T(8,128)(2,1)S(1)} %convolution_convert_fusion.1), channel_id=1, source_target_pairs={{0,1},{1,0},{2,3},{3,2},{4,5},{5,4},{6,7},{7,6},{8,9},{9,8},{10,11... | collective-permute-start | bytes 786440 | tf_op jit(solution)/shard_map/ppermute | solution.py:242
  49.7 1.0 %copy-start.3 = (bf16[128,1024]{1,0:T(8,128)(2,1)S(1)}, bf16[128,1024]{1,0:T(8,128)(2,1)}, u32[]{:S(2)}) copy-start(bf16[128,1024]{1,0:T(8,128)(2,1)} %attend.3) | copy-start | bytes 786436

commit v3 on v2

--- a/solution.py
+++ b/solution.py
@@ -6,6 +6,7 @@
 from jax.experimental import pallas as pl
 from jax.experimental.pallas import tpu as pltpu
 from jax.sharding import PartitionSpec as P
+
 
 HD = 64
 KB = 32
@@ -185,13 +186,16 @@
         return lax.ppermute(x, "kv", [(i, i ^ step) for i in range(n_kv)])
 
     def project(w):
-        return jnp.dot(hidden_rows, w, preferred_element_type=jnp.float32).astype(jnp.bfloat16)
+        return jnp.dot(hidden_rows, w, preferred_element_type=jnp.float32).astype(
+            jnp.bfloat16
+        )
 
     here = lax.axis_index("tp")
-    wo_parts = [
-        lax.dynamic_slice_in_dim(proj_output, lax.rem(here + d, n_tp) * part, part, axis=1)
-        for d in range(n_tp)
-    ]
+
+    def wo_cols(w, d):
+        return lax.dynamic_slice_in_dim(w, lax.rem(here + d, n_tp) * part, part, axis=1)
+
+    wo_parts = [wo_cols(proj_output, d) for d in range(1, n_tp)]
     queries = project(proj_query)
     keys = project(proj_key)
     values = project(proj_value)
@@ -202,7 +206,7 @@
         (near, table, keys, values, queries, *wo_parts)
     )
     far = swap(near, steps[-1])
-    per = 2 if query_blocks % 2 == 0 else 1
+    per = 3 if query_blocks % 3 == 0 else 1
     rows = per * QB
     atts, pieces, sent = [], [], []
     group_rows = heads_w // HD // (kw // HD) * QB
@@ -235,7 +239,7 @@
         atts.append(att)
         got, sends = [], []
         for d in range(1, n_tp):
-            send = jnp.dot(att, wo_parts[d], preferred_element_type=jnp.float32).astype(
+            send = jnp.dot(att, wo_parts[d - 1], preferred_element_type=jnp.float32).astype(
                 jnp.bfloat16
             )
             pairs = [(i, (i + d) % n_tp) for i in range(n_tp)]
@@ -250,10 +254,11 @@
             out = out + piece.astype(jnp.float32)
         return out.astype(jnp.bfloat16)
 
-    own = [
-        jnp.dot(att, wo_parts[0], preferred_element_type=jnp.float32).astype(jnp.bfloat16)
-        for att in atts
-    ]
+    wo_late, *atts = lax.optimization_barrier((proj_output, *atts))
+    own_all = jnp.dot(
+        jnp.concatenate(atts, axis=0), wo_cols(wo_late, 0), preferred_element_type=jnp.float32
+    ).astype(jnp.bfloat16)
+    own = [own_all[i * rows : (i + 1) * rows] for i in range(len(atts))]
     sums = [total(o, g) for o, g in zip(own[:-1], pieces[:-1])]
     out = jnp.concatenate(sums + [own[-1]], axis=0)
     out, last = lax.optimization_barrier((out, own[-1]))

time: 57.1 us -> 56.5 us (0.989)
  waiting for transfers between devices: 7.21 us -> 12.1 us
  local copies, waits for them, and re-layouts: 5.19 us -> 2.51 us
  Pallas kernels: 18.3 us -> 16.6 us
  starting transfers between devices: 11.1 us -> 9.7 us
    ppermute x3 -> x2, waiting for transfers between devices: 3.88 us -> 6.51 us  [local(): got.append(lax.ppermute(send, 'tp', pairs))]
    dynamic_slice x1, local copies, waits for them, and re-layouts: 4 us -> 1.76 us  [wo_cols(): lax.dynamic_slice_in_dim(w, lax.rem(here + d, n_tp) * part, part, axis=1)]
    ppermute x4, waiting for transfers between devices: 3.33 us -> 5.55 us  [swap(): return lax.ppermute(x, 'kv', [(i, i ^ step) for i in range(n_kv)])]
    pallas_call x3 -> x2, Pallas kernels: 13.6 us -> 11.9 us  [local(): pl.pallas_call(functools.partial(attend_kernel, first=chunk * per, count=...]
    ppermute x3 -> x2, starting transfers between devices: 3.72 us -> 2.28 us  [local(): got.append(lax.ppermute(send, 'tp', pairs))]
    unnamed x24 -> x18, local copies, waits for them, and re-layouts: 1.19 us -> 0.73 us
    dot_general x6 -> x3, matrix products: 5.67 us -> 5.79 us  [the longest x2 3.22 us: local(): jnp.dot(att, wo_parts[d - 1], preferred_element_type=jnp.float32)]
  transfers between devices with their start and end apart: 7 -> 6, of which waited for: 3 -> 3; matrix products, arithmetic and copies ran while one was open for 29% -> 26% of each run, Pallas kernels for 19% -> 13%
where the time goes in v3:
time: 56.5 us; the launch traced here: 56.1 us
  Pallas kernels  16.6 us (29%)
  matrix products  13.1 us (23%)
  waiting for transfers between devices  12.1 us (21%)
  starting transfers between devices  9.7 us (17%)
  local copies, waits for them, and re-layouts  2.51 us (4%)
  other arithmetic  1.99 us (4%)
    pallas_call x2, Pallas kernels, local(): pl.pallas_call(functools.partial(attend_kernel, first=chunk * per, count=...  11.9 us
    ppermute x4, starting transfers between devices, swap(): return lax.ppermute(x, 'kv', [(i, i ^ step) for i in range(n_kv)])  7.43 us
    dot_general x3, matrix products, project(): jnp.dot(hidden_rows, w, preferred_element_type=jnp.float32)  7.3 us
    ppermute x2, waiting for transfers between devices, local(): got.append(lax.ppermute(send, 'tp', pairs))  6.51 us
    ppermute x4, waiting for transfers between devices, swap(): return lax.ppermute(x, 'kv', [(i, i ^ step) for i in range(n_kv)])  5.55 us
    pallas_call x1, Pallas kernels, local(): pl.pallas_call(functools.partial(slot_kernel, own_blocks=own_blocks), out...  3.29 us
    dot_general x2, matrix products, local(): jnp.dot(att, wo_parts[d - 1], preferred_element_type=jnp.float32)  3.22 us
    dot_general x1, matrix products, local(): jnp.dot(jnp.concatenate(atts, axis=0), wo_cols(wo_late, 0), preferred_ele...  2.57 us
  transfers between devices with their start and end apart: 6, of which 3 were waited for; matrix products, arithmetic and copies ran while one was open for 26% of the time, Pallas kernels for 13%

profile of v3, /device:TPU:0, one launch (start us, length us, event | category | flops | bytes accessed | tf_op | source)
XLA Modules:
  0.0 56.1 jit_solution(5693134187919661913)
XLA Ops:
  0.0 3.3 %slot_rows.1 = bf16[64,256]{1,0:T(8,128)(2,1)} custom-call(s32[16]{0:T(128)} %hot.7, bf16[384,2048]{1,0:T(8,128)(2,1)} %hidden.1, bf16[2048,128]{1,0:T(8,128)(2,1)} %wk.1, bf16[2048,128]{1,0:T(8,128)(2,1)} %wv.1), custom_call_target="tpu_custom_call" | custom-call | tf_op jit(solution)/shard_map/slot_rows/pallas_call | solution.py:166
  3.3 3.1 %collective-permute-start = (bf16[64,256]{1,0:T(8,128)(2,1)}, bf16[64,256]{1,0:T(8,128)(2,1)S(1)}, u32[]{:S(2)}, u32[]{:S(2)}) collective-permute-start(bf16[64,256]{1,0:T(8,128)(2,1)} %slot_rows.1), channel_id=1, source_target_pairs={{0,4},{2,6},{4,0},{6,2},{8,12},{10,14},{12,8},{14,10},{16,20},{18,... | collective-permute-start | bytes 98312 | tf_op jit(solution)/shard_map/ppermute | solution.py:186
  6.4 4.9 %convolution_convert_fusion.q = bf16[384,1024]{1,0:T(8,128)(2,1)} fusion(bf16[384,2048]{1,0:T(8,128)(2,1)S(1)} %copy-done, bf16[2048,1024]{1,0:T(8,128)(2,1)} %param.9), kind=kOutput, calls=%fused_computation.3 | convolution fusion | flops 1611005952 | bytes 6553600 | tf_op jit(solution)/shard_map/dot_general | solution.py:189
  11.2 1.2 %convolution_convert_fusion.4.keys = bf16[384,128]{1,0:T(8,128)(2,1)} fusion(bf16[384,2048]{1,0:T(8,128)(2,1)S(1)} %copy-done, bf16[2048,128]{1,0:T(8,128)(2,1)S(1)} %copy-done.2), kind=kOutput, calls=%fused_computation.7 | convolution fusion | flops 201375744 | bytes 2195456 | tf_op jit(solution)/shard_map/dot_general | solution.py:189
  12.5 1.6 %collective-permute-start.1 = (bf16[128,256]{1,0:T(8,128)(2,1)S(1)}, bf16[128,256]{1,0:T(8,128)(2,1)S(1)}, u32[]{:S(2)}, u32[]{:S(2)}) collective-permute-start(bf16[128,256]{1,0:T(8,128)(2,1)S(1)} %pad_maximum_fusion.3), channel_id=1, source_target_pairs={{0,8},{2,10},{4,12},{6,14},{8,0},{10,2},{12,4},{14,6},{16,24},{18,... | collective-permute-start | bytes 196616 | tf_op jit(solution)/shard_map/ppermute | solution.py:186
  14.1 1.2 %convolution_convert_fusion.3.values = bf16[384,128]{1,0:T(8,128)(2,1)} fusion(bf16[384,2048]{1,0:T(8,128)(2,1)S(1)} %copy-done, bf16[2048,128]{1,0:T(8,128)(2,1)S(1)} %copy-done.3), kind=kOutput, calls=%fused_computation.6 | convolution fusion | flops 201375744 | bytes 2195456 | tf_op jit(solution)/shard_map/dot_general | solution.py:189
  15.3 1.4 %table.1 = s32[16]{0:T(128)} custom-call(s32[16]{0:T(128)} %hot.7), custom_call_target="tpu_custom_call" | custom-call | tf_op jit(solution)/shard_map/table/pallas_call | solution.py:177
  16.8 2.7 %collective-permute-start.2 = (bf16[256,256]{1,0:T(8,128)(2,1)S(1)}, bf16[256,256]{1,0:T(8,128)(2,1)S(1)}, u32[]{:S(2)}, u32[]{:S(2)}) collective-permute-start(bf16[256,256]{1,0:T(8,128)(2,1)S(1)} %pad_maximum_fusion.2), channel_id=1, source_target_pairs={{0,16},{2,18},{4,20},{6,22},{8,24},{10,26},{12,28},{14,30},{16,0},... | collective-permute-start | bytes 393224 | tf_op jit(solution)/shard_map/ppermute | solution.py:186
  19.5 1.8 %constant_dynamic-slice_fusion = bf16[1024,1024]{1,0:T(8,128)(2,1)S(1)} fusion(bf16[1024,2048]{1,0:T(8,128)(2,1)} %param.12, s32[]{:T(128)S(6)} %select_n.6), kind=kLoop, calls=%fused_computation.19 | loop fusion | bytes 4194308 | tf_op jit(solution)/shard_map/dynamic_slice | solution.py:196
  21.3 4.0 %collective-permute-done.2 = bf16[256,256]{1,0:T(8,128)(2,1)S(1)} collective-permute-done((bf16[256,256]{1,0:T(8,128)(2,1)S(1)}, bf16[256,256]{1,0:T(8,128)(2,1)S(1)}, u32[]{:S(2)}, u32[]{:S(2)}) %collective-permute-start.2) | collective-permute-done | bytes 131104 | tf_op jit(solution)/shard_map/ppermute | solution.py:186
  25.3 0.1 collective-permute-start.3
  25.4 1.5 %collective-permute-done.3.far = bf16[512,256]{1,0:T(8,128)(2,1)S(1)} collective-permute-done((bf16[512,256]{1,0:T(8,128)(2,1)S(1)}, bf16[512,256]{1,0:T(8,128)(2,1)S(1)}, u32[]{:S(2)}, u32[]{:S(2)}) %collective-permute-start.3) | collective-permute-done | bytes 262176 | tf_op jit(solution)/shard_map/ppermute | solution.py:186
  26.9 0.7 %copy-done.7 = bf16[512,256]{1,0:T(8,128)(2,1)} copy-done((bf16[512,256]{1,0:T(8,128)(2,1)}, bf16[512,256]{1,0:T(8,128)(2,1)S(1)}, u32[]{:S(2)}) %copy-start.7) | copy-done | bytes 262168
  27.6 5.9 %attend.2 = bf16[192,1024]{1,0:T(8,128)(2,1)} custom-call(s32[6,16]{1,0:T(8,128)} %codes.3, s32[16]{0:T(128)} %hot.7, s32[16]{0:T(128)} %table.1, f32[16]{0:T(128)} %scale.3, bf16[384,1024]{1,0:T(8,128)(2,1)} %convolution_convert_fusion.q, bf16[384,128]{1,0:T(8,128)(2,1)} %convolution_convert_fusion.4.keys, ...), custom_call_target="tpu_custom_call" | custom-call | tf_op jit(solution)/shard_map/attend/pallas_call | solution.py:214
  33.6 1.6 %convolution_convert_fusion.2.rest_0_ = bf16[192,1024]{1,0:T(8,128)(2,1)S(1)} fusion(bf16[192,1024]{1,0:T(8,128)(2,1)} %attend.2, bf16[1024,1024]{1,0:T(8,128)(2,1)S(1)} %constant_dynamic-slice_fusion), kind=kOutput, calls=%fused_computation.5 | convolution fusion | flops 402849792 | bytes 2883584 | tf_op jit(solution)/shard_map/dot_general | solution.py:242
  35.2 1.5 %collective-permute-start.4 = (bf16[192,1024]{1,0:T(8,128)(2,1)S(1)}, bf16[192,1024]{1,0:T(8,128)(2,1)S(1)}, u32[]{:S(2)}, u32[]{:S(2)}) collective-permute-start(bf16[192,1024]{1,0:T(8,128)(2,1)S(1)} %convolution_convert_fusion.2.rest_0_), channel_id=1, source_target_pairs={{0,1},{1,0},{2,3},{3,2},{4,5},{5,4},{6,7},{7,6},{8,9},{9,8},{10,11... | collective-permute-start | bytes 1179656 | tf_op jit(solution)/shard_map/ppermute | solution.py:246
  36.7 6.0 %attend.3 = bf16[192,1024]{1,0:T(8,128)(2,1)} custom-call(s32[6,16]{1,0:T(8,128)} %codes.3, s32[16]{0:T(128)} %hot.7, s32[16]{0:T(128)} %table.1, f32[16]{0:T(128)} %scale.3, bf16[384,1024]{1,0:T(8,128)(2,1)} %convolution_convert_fusion.q, bf16[384,128]{1,0:T(8,128)(2,1)} %convolution_convert_fusion.4.keys, ...), custom_call_target="tpu_custom_call" | custom-call | tf_op jit(solution)/shard_map/attend/pallas_call | solution.py:214
  42.7 1.6 %convolution_convert_fusion.1 = bf16[192,1024]{1,0:T(8,128)(2,1)S(1)} fusion(bf16[192,1024]{1,0:T(8,128)(2,1)} %attend.3, bf16[1024,1024]{1,0:T(8,128)(2,1)S(1)} %constant_dynamic-slice_fusion), kind=kOutput, calls=%fused_computation.4 | convolution fusion | flops 402849792 | bytes 2883584 | tf_op jit(solution)/shard_map/dot_general | solution.py:242
  44.3 0.7 %collective-permute-start.5 = (bf16[192,1024]{1,0:T(8,128)(2,1)S(1)}, bf16[192,1024]{1,0:T(8,128)(2,1)S(1)}, u32[]{:S(2)}, u32[]{:S(2)}) collective-permute-start(bf16[192,1024]{1,0:T(8,128)(2,1)S(1)} %convolution_convert_fusion.1), channel_id=1, source_target_pairs={{0,1},{1,0},{2,3},{3,2},{4,5},{5,4},{6,7},{7,6},{8,9},{9,8},{10,11... | collective-permute-start | bytes 1179656 | tf_op jit(solution)/shard_map/ppermute | solution.py:246
  45.1 2.6 %fusion.2 = bf16[384,1024]{1,0:T(8,128)(2,1)S(1)} fusion(bf16[1024,2048]{1,0:T(8,128)(2,1)} %param.12, s32[]{:T(128)S(6)} %select_n.7, bf16[192,1024]{1,0:T(8,128)(2,1)S(1)} %copy-done.5, bf16[192,1024]{1,0:T(8,128)(2,1)S(1)} %copy-done.6), kind=kOutput, calls=%fused_computation.2 | convolution fusion | flops 807272448 | bytes 3670020 | tf_op jit(solution)/shard_map/dot_general | solution.py:258
  47.7 0.1 add_convert_fusion.1
  47.8 0.9 %pad_maximum_fusion = bf16[384,1024]{1,0:T(8,128)(2,1)} fusion(bf16[192,1024]{1,0:T(8,128)(2,1)S(1)} %slice.9, bf16[192,1024]{1,0:T(8,128)(2,1)S(1)} %add_convert_fusion.1), kind=kLoop, calls=%fused_computation.11 | loop fusion | flops 1572864 | bytes 1572864 | tf_op jit(solution)/shard_map/concatenate | solution.py:263
  48.8 6.5 %collective-permute-done.5 = bf16[192,1024]{1,0:T(8,128)(2,1)S(1)} collective-permute-done((bf16[192,1024]{1,0:T(8,128)(2,1)S(1)}, bf16[192,1024]{1,0:T(8,128)(2,1)S(1)}, u32[]{:S(2)}, u32[]{:S(2)}) %collective-permute-start.5) | collective-permute-done | bytes 393248 | tf_op jit(solution)/shard_map/ppermute | solution.py:246
  55.3 0.9 %fusion.8 = bf16[384,1024]{1,0:T(8,128)(2,1)} fusion(bf16[384,1024]{1,0:T(8,128)(2,1)} %pad_maximum_fusion, bf16[192,1024]{1,0:T(8,128)(2,1)S(1)} %collective-permute-done.5, bf16[192,1024]{1,0:T(8,128)(2,1)S(1)} %slice.9), kind=kLoop, calls=%fused_computation.14 | loop fusion | flops 786432 | bytes 1179648 | tf_op jit(solution)/shard_map/dynamic_update_slice | solution.py:265
  (24 shorter events, 0.1 us)
Async XLA Ops:
  0.0 6.4 %copy-start = (bf16[384,2048]{1,0:T(8,128)(2,1)S(1)}, bf16[384,2048]{1,0:T(8,128)(2,1)}, u32[]{:S(2)}) copy-start(bf16[384,2048]{1,0:T(8,128)(2,1)} %hidden.1) | copy-start | bytes 4718596
  3.3 7.9 %copy-start.2 = (bf16[2048,128]{1,0:T(8,128)(2,1)S(1)}, bf16[2048,128]{1,0:T(8,128)(2,1)}, u32[]{:S(2)}) copy-start(bf16[2048,128]{1,0:T(8,128)(2,1)} %wk.1) | copy-start | bytes 1572868
  3.3 9.2 %collective-permute-start = (bf16[64,256]{1,0:T(8,128)(2,1)}, bf16[64,256]{1,0:T(8,128)(2,1)S(1)}, u32[]{:S(2)}, u32[]{:S(2)}) collective-permute-start(bf16[64,256]{1,0:T(8,128)(2,1)} %slot_rows.1), channel_id=1, source_target_pairs={{0,4},{2,6},{4,0},{6,2},{8,12},{10,14},{12,8},{14,10},{16,20},{18,... | collective-permute-start | bytes 98312 | tf_op jit(solution)/shard_map/ppermute | solution.py:186
  11.2 1.2 %copy-start.8 = (bf16[64,256]{1,0:T(8,128)(2,1)S(1)}, bf16[64,256]{1,0:T(8,128)(2,1)}, u32[]{:S(2)}) copy-start(bf16[64,256]{1,0:T(8,128)(2,1)} %slot_rows.1) | copy-start | bytes 98308
  11.2 2.9 %copy-start.3 = (bf16[2048,128]{1,0:T(8,128)(2,1)S(1)}, bf16[2048,128]{1,0:T(8,128)(2,1)}, u32[]{:S(2)}) copy-start(bf16[2048,128]{1,0:T(8,128)(2,1)} %wv.1) | copy-start | bytes 1572868
  12.5 4.3 %collective-permute-start.1 = (bf16[128,256]{1,0:T(8,128)(2,1)S(1)}, bf16[128,256]{1,0:T(8,128)(2,1)S(1)}, u32[]{:S(2)}, u32[]{:S(2)}) collective-permute-start(bf16[128,256]{1,0:T(8,128)(2,1)S(1)} %pad_maximum_fusion.3), channel_id=1, source_target_pairs={{0,8},{2,10},{4,12},{6,14},{8,0},{10,2},{12,4},{14,6},{16,24},{18,... | collective-permute-start | bytes 196616 | tf_op jit(solution)/shard_map/ppermute | solution.py:186
  16.8 8.4 %collective-permute-start.2 = (bf16[256,256]{1,0:T(8,128)(2,1)S(1)}, bf16[256,256]{1,0:T(8,128)(2,1)S(1)}, u32[]{:S(2)}, u32[]{:S(2)}) collective-permute-start(bf16[256,256]{1,0:T(8,128)(2,1)S(1)} %pad_maximum_fusion.2), channel_id=1, source_target_pairs={{0,16},{2,18},{4,20},{6,22},{8,24},{10,26},{12,28},{14,30},{16,0},... | collective-permute-start | bytes 393224 | tf_op jit(solution)/shard_map/ppermute | solution.py:186
  25.3 1.6 %copy-start.1 = (bf16[512,256]{1,0:T(8,128)(2,1)}, bf16[512,256]{1,0:T(8,128)(2,1)S(1)}, u32[]{:S(2)}) copy-start(bf16[512,256]{1,0:T(8,128)(2,1)S(1)} %pad_maximum_fusion.1.near) | copy-start | bytes 786436
  25.3 1.6 %collective-permute-start.3 = (bf16[512,256]{1,0:T(8,128)(2,1)S(1)}, bf16[512,256]{1,0:T(8,128)(2,1)S(1)}, u32[]{:S(2)}, u32[]{:S(2)}) collective-permute-start(bf16[512,256]{1,0:T(8,128)(2,1)S(1)} %pad_maximum_fusion.1.near), channel_id=1, source_target_pairs={{0,2},{2,0},{4,6},{6,4},{8,10},{10,8},{12,14},{14,12},{16,18},{18,... | collective-permute-start | bytes 786440 | tf_op jit(solution)/shard_map/ppermute | solution.py:186
  26.9 0.7 %copy-start.7 = (bf16[512,256]{1,0:T(8,128)(2,1)}, bf16[512,256]{1,0:T(8,128)(2,1)S(1)}, u32[]{:S(2)}) copy-start(bf16[512,256]{1,0:T(8,128)(2,1)S(1)} %collective-permute-done.3.far) | copy-start | bytes 786436
  35.1 1.6 %copy-start.4 = (bf16[192,1024]{1,0:T(8,128)(2,1)}, bf16[192,1024]{1,0:T(8,128)(2,1)S(1)}, u32[]{:S(2)}) copy-start(bf16[192,1024]{1,0:T(8,128)(2,1)S(1)} %convolution_convert_fusion.2.rest_0_) | copy-start | bytes 1179652
  35.1 9.9 %copy-start.6 = (bf16[192,1024]{1,0:T(8,128)(2,1)S(1)}, bf16[192,1024]{1,0:T(8,128)(2,1)}, u32[]{:S(2)}) copy-start(bf16[192,1024]{1,0:T(8,128)(2,1)} %attend.2) | copy-start | bytes 1179652
  35.2 12.5 %collective-permute-start.4 = (bf16[192,1024]{1,0:T(8,128)(2,1)S(1)}, bf16[192,1024]{1,0:T(8,128)(2,1)S(1)}, u32[]{:S(2)}, u32[]{:S(2)}) collective-permute-start(bf16[192,1024]{1,0:T(8,128)(2,1)S(1)} %convolution_convert_fusion.2.rest_0_), channel_id=1, source_target_pairs={{0,1},{1,0},{2,3},{3,2},{4,5},{5,4},{6,7},{7,6},{8,9},{9,8},{10,11... | collective-permute-start | bytes 1179656 | tf_op jit(solution)/shard_map/ppermute | solution.py:246
  42.7 2.4 %copy-start.5 = (bf16[192,1024]{1,0:T(8,128)(2,1)S(1)}, bf16[192,1024]{1,0:T(8,128)(2,1)}, u32[]{:S(2)}) copy-start(bf16[192,1024]{1,0:T(8,128)(2,1)} %attend.3) | copy-start | bytes 1179652
  44.3 10.9 %collective-permute-start.5 = (bf16[192,1024]{1,0:T(8,128)(2,1)S(1)}, bf16[192,1024]{1,0:T(8,128)(2,1)S(1)}, u32[]{:S(2)}, u32[]{:S(2)}) collective-permute-start(bf16[192,1024]{1,0:T(8,128)(2,1)S(1)} %convolution_convert_fusion.1), channel_id=1, source_target_pairs={{0,1},{1,0},{2,3},{3,2},{4,5},{5,4},{6,7},{7,6},{8,9},{9,8},{10,11... | collective-permute-start | bytes 1179656 | tf_op jit(solution)/shard_map/ppermute | solution.py:246
